TPU v7x, 128 devices: a whole 4x4x4 slice. The times are simulated.
128 devices in a mesh: sp: 16 (over z, y), tp: 8 (over x, core).
Axes of the slice: x: 4, y: 4, z: 4, core: 2. Of those that a mesh axis runs over, the one named last changes fastest.
Arguments:
- tokens: bfloat16 [4, 8192, 1024], P(None, ('sp', 'tp')), may hold values from -6 to 6
- norm_gain: float32 [1024], replicated, may hold values from 0.1 to 1.9
- x_weight: bfloat16 [1024, 1024], P('sp', 'tp'), may hold values from -0.1875 to 0.1875
- z_weight: bfloat16 [1024, 1024], P('sp', 'tp'), may hold values from -0.1875 to 0.1875
- b_weight: bfloat16 [1024, 1024], P('sp', 'tp'), may hold values from -0.1875 to 0.1875
- c_weight: bfloat16 [1024, 1024], P('sp', 'tp'), may hold values from -0.1875 to 0.1875
- dt_weight: bfloat16 [1024, 16], P('sp', 'tp'), may hold values from -0.1875 to 0.1875
- x_conv: float32 [4, 1024], P(None, 'tp'), may hold values from -3 to 3
- b_conv: float32 [4, 1024], P(None, 'tp'), may hold values from -3 to 3
- c_conv: float32 [4, 1024], P(None, 'tp'), may hold values from -3 to 3
- dt_bias: float32 [16], P('tp'), may hold values from -1 to 1
- decay_rate: float32 [16], P('tp'), may hold values from 0.15 to 3.5
- out_gain: float32 [1024], P('tp'), may hold values from 0.1 to 1.9
- out_weight: bfloat16 [1024, 1024], P('tp', 'sp'), may hold values from -0.1875 to 0.1875
Outputs:
- mixed: bfloat16 [4, 8192, 1024], P(None, ('sp', 'tp'))
All inputs are finite; a program needn't handle non-finite values.
Results may differ from a plain program's by a relative error of at most 0.02.
Values may be sent and summed in bfloat16 or wider, within the bound.
A program may use at most 64 MiB of HBM per device.

v0:
```python
import jax
import jax.numpy as jnp
from jax import lax
from jax.sharding import Mesh
from jax.sharding import PartitionSpec as P

HEADS = 16
HEAD_P = 64
STATE = 128
GROUPS = 8
CONV = 4
BLOCK = 32
SP = ("sp_0", "sp_1")
TP = ("tp_0", "tp_1")
SP_TP = ("sp_0", "sp_1", "tp_0", "tp_1")


epsilon = 1e-05
precise = lax.Precision.DEFAULT


def laid_out(parts, dim):
    dims = list(parts.shape[1:])
    dims[dim] *= parts.shape[0]
    return jnp.moveaxis(parts, 0, dim).reshape(dims)


def one_gather(arrays, axis, dims):
    ravelled = jnp.concatenate([a.reshape(-1) for a in arrays])
    lines, at, done = lax.all_gather(ravelled, axis), 0, []
    for a, dim in zip(arrays, dims):
        parts = lines[:, at : at + a.size].reshape(-1, *a.shape)
        done.append(laid_out(parts, dim))
        at += a.size
    return tuple(done)


def over_all(value, axis, dim, block):
    whole = lax.all_gather(value, axis, axis=dim, tiled=True)
    return block(whole, jnp.int32(0))


def shortened(value):
    def short(part):
        return part.astype(jnp.bfloat16) if part.dtype == jnp.float32 else part

    return jax.tree.map(short, value)


def from_behind(block, axis, distance):
    devices = range(lax.axis_size(axis))
    route = [(i - distance, i) for i in devices if i - distance in devices]
    return lax.ppermute(block, axis, route)


def filled_with(value, identity):
    return jax.tree.map(
        lambda part, zero: jnp.zeros_like(part) + jnp.asarray(zero, part.dtype), value, identity
    )


def prefix_by_axis(value, axes, combine, identity, reverse):
    before = start = filled_with(value, identity)
    total = value
    for axis in reversed(axes):
        peers, index = lax.axis_size(axis), lax.axis_index(axis)
        pieces = jax.tree.map(lambda part: lax.all_gather(part, axis), total)
        inside, total = start, start
        for k in reversed(range(peers)) if reverse else range(peers):
            passed = k > index if reverse else k < index
            total = combine(total, jax.tree.map(lambda part: part[k], pieces))
            inside = jax.tree.map(lambda new, old: jnp.where(passed, new, old), total, inside)
        before = combine(inside, before)
    return before


def gather_axes(value, axes, dim):
    for axis in reversed(axes):
        value = lax.all_gather(value, axis, axis=dim, tiled=True)
    return value


def cut_rows(length, count):
    unit = 8 if length >= 8 * count else 1
    return [length // unit * k // count * unit for k in range(1, count)]


def gather_in_order(value, axes, turns):
    parts = value
    for k in turns:
        parts = lax.all_gather(parts, axes[k])
    done = turns[::-1]
    back = [done.index(k) for k in range(len(axes))]
    parts = parts.transpose(*back, *range(len(axes), parts.ndim))
    return parts.reshape(-1, *value.shape)


def spread_gather(value, axes, dim):
    numbers = list(range(len(axes)))[::-1]
    split_at = value.shape.index(max(value.shape[:-1] or value.shape))
    edges = [0, *cut_rows(value.shape[split_at], len(axes)), value.shape[split_at]]
    done = []
    for k, (start, end) in enumerate(zip(edges, edges[1:])):
        if end > start:
            slab = lax.slice_in_dim(value, start, end, axis=split_at)
            done.append(gather_in_order(slab, axes, numbers[k:] + numbers[:k]))
    return laid_out(jnp.concatenate(done, axis=split_at + 1), dim)


def block_pass(inputs_dt, logdecay, b_state, c_state, per_group):
    seq_count, span_len, head_count, head_width = inputs_dt.shape
    groups, state_width = (b_state.shape[2], b_state.shape[3])
    blocks = span_len // BLOCK
    x_blocks = inputs_dt.reshape(seq_count, blocks, BLOCK, groups, per_group, head_width)
    b_blocks = b_state.reshape(seq_count, blocks, BLOCK, groups, state_width)
    c_blocks = c_state.reshape(seq_count, blocks, BLOCK, groups, state_width)
    log_blocks = logdecay.reshape(seq_count, blocks, BLOCK, groups, per_group)
    within = jnp.moveaxis(jnp.cumsum(log_blocks, axis=2), 2, -1)
    scores = jnp.einsum("sclgn,scmgn->scglm", c_blocks, b_blocks, precision=precise)
    lower_mask = jnp.tril(jnp.ones((BLOCK, BLOCK), dtype=bool))
    log_gaps = jnp.where(lower_mask, within[..., :, None] - within[..., None, :], -jnp.inf)
    weights = scores[:, :, :, None] * jnp.exp(log_gaps)
    diagonal_part = jnp.einsum("scghlm,scmghp->sclghp", weights, x_blocks, precision=precise)
    end_decay = jnp.moveaxis(jnp.exp(within[..., -1:] - within), -1, 2)
    block_states = jnp.einsum(
        "sclgn,sclghp->scghpn", b_blocks, x_blocks * end_decay[..., None], precision=precise
    )
    block_decay = jnp.exp(within[..., -1])

    def advance(running_state, inputs):
        fresh_state, shrink = inputs
        return (running_state * shrink[..., None, None] + fresh_state, running_state)

    start_state = jnp.zeros((seq_count, groups, per_group, head_width, state_width), jnp.float32)
    final_state, entering = lax.scan(
        advance, start_state, (jnp.moveaxis(block_states, 1, 0), jnp.moveaxis(block_decay, 1, 0))
    )
    entering = jnp.moveaxis(entering, 0, 1)
    start_decay = jnp.moveaxis(jnp.exp(within), -1, 2)
    carried_part = (
        jnp.einsum("sclgn,scghpn->sclghp", c_blocks, entering, precision=precise)
        * start_decay[..., None]
    )
    return (
        (diagonal_part + carried_part).reshape(seq_count, span_len, head_count, head_width),
        final_state,
    )


def combine(earlier, latter):
    return (earlier[0] * latter[0], earlier[1] * latter[0][:, :, None, None] + latter[1])


def local(
    tokens,
    norm_gain,
    x_weight,
    z_weight,
    b_weight,
    c_weight,
    dt_weight,
    x_conv,
    b_conv,
    c_conv,
    dt_bias,
    decay_rate,
    out_gain,
    out_weight,
):
    seq_count = tokens.shape[0]
    source = tokens.astype(jnp.float32)
    normed = (
        source * lax.rsqrt(jnp.mean(source * source, axis=-1, keepdims=True) + epsilon) * norm_gain
    ).astype(jnp.bfloat16)
    full_x, full_b, full_c, full_z, full_dt = one_gather(
        (x_weight, b_weight, c_weight, z_weight, dt_weight), SP, (0, 0, 0, 0, 0)
    )

    def project(shard_rows, first_row):
        flattened = shard_rows.reshape(-1, shard_rows.shape[-1])
        pieces_out = [
            jnp.dot(flattened, weight, preferred_element_type=jnp.float32).astype(jnp.bfloat16)
            for weight in (full_x, full_b, full_c, full_z, full_dt)
        ]
        return jnp.concatenate(pieces_out, axis=1).reshape(
            shard_rows.shape[0], shard_rows.shape[1], -1
        )

    projected = over_all(normed, TP, 1, project)
    inner_dev = x_weight.shape[1]
    state_dev = b_weight.shape[1]
    heads_dev = dt_weight.shape[1]
    span_len = projected.shape[1]
    conv_width = inner_dev + 2 * state_dev
    conv_input = projected[:, :, :conv_width]
    z_proj = projected[:, :, conv_width : conv_width + inner_dev]
    dt_raw = projected[:, :, conv_width + inner_dev :]
    tail_rows = conv_input[:, span_len - (CONV - 1) :, :]
    before_rows = from_behind(shortened(tail_rows), SP, 1).astype(tail_rows.dtype)
    taps = jnp.concatenate([x_conv, b_conv, c_conv], axis=1)
    extended = jnp.concatenate([before_rows, conv_input], axis=1).astype(jnp.float32)
    running = jnp.zeros((seq_count, span_len, conv_width), jnp.float32)
    for offset in range(CONV):
        running = running + taps[offset] * extended[:, offset : offset + span_len]
    conv_out = jax.nn.silu(running)
    x_conv_out = conv_out[..., :inner_dev].reshape(seq_count, span_len, heads_dev, HEAD_P)
    b_state = conv_out[..., inner_dev : inner_dev + state_dev].reshape(
        seq_count, span_len, -1, STATE
    )
    c_state = conv_out[..., inner_dev + state_dev :].reshape(seq_count, span_len, -1, STATE)
    groups_dev = b_state.shape[2]
    length = span_len * lax.axis_size(SP)
    step_dt = jax.nn.softplus(dt_raw.astype(jnp.float32) + dt_bias)
    logdecay = -(step_dt * decay_rate) / length
    per_group = HEADS // GROUPS
    y_local, final_state = block_pass(
        x_conv_out * step_dt[..., None], logdecay, b_state, c_state, per_group
    )
    seg_cum = jnp.cumsum(logdecay, axis=1)
    seg_decay = jnp.exp(jnp.sum(logdecay, axis=1))
    seg_state = final_state.reshape(seq_count, heads_dev, HEAD_P, STATE)

    def finish(incoming, lower_seq, upper_seq):
        picked = upper_seq - lower_seq
        shaped = incoming.reshape(picked, groups_dev, per_group, HEAD_P, STATE)
        carried = jnp.einsum(
            "slgn,sghpn->slghp", c_state[lower_seq:upper_seq], shaped, precision=precise
        )
        carried = (
            carried.reshape(picked, span_len, heads_dev, HEAD_P)
            * jnp.exp(seg_cum[lower_seq:upper_seq])[..., None]
        )
        y_all = y_local[lower_seq:upper_seq] + carried
        gate_act = jax.nn.silu(z_proj[lower_seq:upper_seq].astype(jnp.float32))
        gated = (y_all.reshape(picked, span_len, inner_dev) * gate_act).reshape(
            picked, span_len, -1, per_group * HEAD_P
        )
        gated = gated * lax.rsqrt(jnp.mean(gated * gated, axis=-1, keepdims=True) + epsilon)
        return (gated.reshape(picked, span_len, inner_dev) * out_gain).astype(jnp.bfloat16)

    incoming = tuple(
        (
            part.astype(kind)
            for part, kind in zip(
                prefix_by_axis(
                    (seg_decay.astype(jnp.bfloat16), seg_state.astype(jnp.bfloat16)),
                    SP,
                    combine,
                    (jnp.ones_like(seg_decay), jnp.zeros_like(seg_state)),
                    False,
                ),
                (jnp.float32, jnp.float32),
            )
        )
    )
    gated_all = finish(incoming[1], 0, seq_count)
    full_out = gather_axes(out_weight, SP, 1)
    own_gated = lax.all_to_all(gated_all, TP, split_axis=1, concat_axis=2, tiled=True)
    whole_out = spread_gather(full_out, TP, 0)
    own_count = own_gated.shape[1]
    product = jnp.dot(
        own_gated.reshape(-1, own_gated.shape[2]), whole_out, preferred_element_type=jnp.float32
    )
    return product.reshape(seq_count, own_count, -1).astype(jnp.bfloat16)


def solution(mesh):
    torus = Mesh(mesh.devices.reshape(4, 4, 4, 2), ("sp_0", "sp_1", "tp_0", "tp_1"))
    return jax.shard_map(
        local,
        mesh=torus,
        in_specs=(
            P(None, SP_TP, None),
            P(),
            P(SP, TP),
            P(SP, TP),
            P(SP, TP),
            P(SP, TP),
            P(SP, TP),
            P(None, TP),
            P(None, TP),
            P(None, TP),
            P(TP),
            P(TP),
            P(TP),
            P(TP, SP),
        ),
        out_specs=P(None, SP_TP, None),
        check_vma=False,
    )
```

profile of v0, /device:TPU:1, one launch (start us, length us, event | category | flops | bytes accessed | tf_op | source)
XLA Modules:
  0.0 289.2 jit_solution(4969118297879955030)
XLA Ops:
  14.6 10.4 %all_gather.62 = bf16[128,256]{0,1:T(8,128)(2,1)S(1)} all-gather(bf16[128,64]{0,1:T(8,128)(2,1)S(1)} %copy-done.9), channel_id=1, replica_groups=mesh['sp_0'=4,'sp_1'=4,'tp_0'=4,'tp_1'=2] {'sp_1'}, dimensions={1}, use_global_device_ids=true | all-gather | bytes 81920 | tf_op jit(solution)/shard_map/all_gather | solution.py:79
  25.0 11.0 %all_gather.63 = bf16[128,1024]{1,0:T(8,128)(2,1)S(1)} all-gather(bf16[128,256]{1,0:T(8,128)(2,1)S(1)} %copy.225), channel_id=1, replica_groups=mesh['sp_0'=4,'sp_1'=4,'tp_0'=4,'tp_1'=2] {'sp_0'}, dimensions={1}, use_global_device_ids=true | all-gather | bytes 327680 | tf_op jit(solution)/shard_map/all_gather | solution.py:79
  36.1 11.1 %all-gather.5 = bf16[256,1024]{1,0:T(8,128)(2,1)} all-gather(bf16[64,1024]{1,0:T(8,128)(2,1)S(1)} %get-tuple-element.131), channel_id=7, replica_groups=mesh['sp_0'=4,'sp_1'=4,'tp_0'=4,'tp_1'=2] {'tp_0'}, dimensions={0}, use_global_device_ids=true | all-gather | bytes 655360 | tf_op jit(solution)/shard_map/all_gather | solution.py:91
  47.2 10.9 %all-gather.3 = bf16[128,1024]{1,0:T(8,128)(2,1)} all-gather(bf16[64,1024]{1,0:T(8,128)(2,1)S(1)} %get-tuple-element.130), channel_id=5, replica_groups=mesh['sp_0'=4,'sp_1'=4,'tp_0'=4,'tp_1'=2] {'tp_1'}, dimensions={0}, use_global_device_ids=true | all-gather | bytes 393216 | tf_op jit(solution)/shard_map/all_gather | solution.py:91
  62.3 30.8 %all-gather.14.cloned.1.call-done = bf16[4,512,1024]{2,1,0:T(8,128)(2,1)} async-done(((bf16[4,64,1024]{2,1,0:T(8,128)(2,1)}), bf16[4,512,1024]{2,1,0:T(8,128)(2,1)}) %all-gather.14.cloned.1.call-update) | async-done | bytes 4194320 | tf_op jit(solution)/shard_map/all_gather | solution.py:39
  93.1 4.7 %fusion.9 = bf16[2048,514]{0,1:T(8,128)(2,1)} fusion(bf16[2048,1024]{1,0:T(8,128)(2,1)} %bitcast.263, bf16[1024,128]{1,0:T(8,128)(2,1)S(1)} %reshape_reshape.17), kind=kOutput, calls=%fused_computation.22 | convolution fusion | flops 537133056 | bytes 4980736 | tf_op jit(solution)/shard_map/dot_general | solution.py:182
  106.6 5.0 %reshape.263 = bf16[4,512,514]{1,0,2:T(4,128)(2,1)S(1)} reshape(bf16[2048,514]{0,1:T(8,128)(2,1)} %fusion.10) | data formatting | bytes 4210688 | tf_op jit(solution)/shard_map/reshape | solution.py:185
  112.7 3.7 %collective-permute-start = (bf16[4,3,384]{2,1,0:T(4,128)(2,1)}, bf16[4,3,384]{2,1,0:T(4,128)(2,1)}, u32[]{:S(2)}, u32[]{:S(2)}) collective-permute-start(bf16[4,3,384]{2,1,0:T(4,128)(2,1)} %copy.233), channel_id=1, source_target_pairs={{0,8},{8,16},{16,24},{24,32},{32,40},{40,48},{48,56},{56,64},{64,7... | collective-permute-start | bytes 27656 | tf_op jit(solution)/shard_map/ppermute | solution.py:53
  125.2 7.9 %all-gather.8 = bf16[4,4,2]{1,2,0:T(2,128)(2,1)S(1)} all-gather(bf16[1,4,2]{1,2,0:T(2,128)(2,1)S(1)} %bitcast.288), channel_id=3, replica_groups=mesh['sp_0'=4,'sp_1'=4,'tp_0'=4,'tp_1'=2] {'sp_1'}, dimensions={0}, use_global_device_ids=true | all-gather | bytes 80 | tf_op jit(solution)/shard_map/all_gather | solution.py:67
  133.1 6.7 %all_gather.59 = bf16[4,4,2]{1,2,0:T(2,128)(2,1)S(1)} all-gather(bf16[1,4,2]{1,2,0:T(2,128)(2,1)S(1)} %get-tuple-element.138), channel_id=1, replica_groups=mesh['sp_0'=4,'sp_1'=4,'tp_0'=4,'tp_1'=2] {'sp_0'}, dimensions={0}, use_global_device_ids=true | all-gather | bytes 80 | tf_op jit(solution)/shard_map/all_gather | solution.py:67
  140.5 2.4 reduce-window.6
  147.0 3.1 %copy.234 = bf16[4,512,384]{2,1,0:T(8,128)(2,1)S(1)} copy(bf16[4,512,384]{1,0,2:T(4,128)(2,1)} %slice.185) | data formatting | bytes 3145728
  166.8 3.3 %reshape.264 = f32[4,16,32,2,64]{4,3,2,1,0:T(2,128)} reshape(f32[4,512,128]{2,1,0:T(8,128)} %slice.193) | data formatting | bytes 2097152 | tf_op jit(solution)/shard_map/reshape | solution.py:206
  170.1 6.1 %convolution_bitcast_fusion = f32[16,4,1,2,64,128]{5,4,3,0,1,2:T(8,128)} fusion(bf16[4,16,32,128,1]{3,2,4,1,0:T(8,128)(2,1)} %bitcast.276, f32[4,16,32,2,64]{4,3,2,1,0:T(2,128)} %reshape.264, f32[4,16,32,2]{2,3,1,0:T(2,128)S(1)} %copy.197, f32[4,16,32,2]{2,3,1,0:T(2,128)} %copy.190), kind=kOutput, calls=%fused_computation.25 | convolution fusion | flops 67633152 | bytes 5799936 | tf_op jit(solution)/shard_map/sclgn,sclghp->scghpn/dot_general | solution.py:125
  176.2 40.0 %while.13 = (s32[]{:T(128)}, f32[4,1,2,64,128]{4,3,2,1,0:T(8,128)S(1)}, bf16[16,4,1,2,64,128]{5,4,3,1,2,0:T(8,128)(2,1)}, f32[16,4,1,2]{1,3,2,0:T(2,128)}, f32[1...) while((s32[]{:T(128)}, f32[4,1,2,64,128]{4,3,2,1,0:T(8,128)S(1)}, ...), condition=%wide.region_3.4_spmd.clone, body=%wide.region_2.3_spmd.clone.sunk | while | flops 262147 | bytes 1179916 | solution.py:135
  217.8 3.7 %fusion.16 = f32[4,16,2,64,32]{3,4,2,1,0:T(8,128)S(1)} fusion(f32[4,16,32,2,64]{4,3,2,1,0:T(2,128)} %reshape.264, f32[4,16,2,32]{3,2,1,0:T(2,128)S(1)} %copy-done.7, f32[4,16,32,32]{3,2,1,0:T(8,128)S(1)} %fusion.105, f32[4,16,32,2]{2,3,1,0:T(2,128)} %copy.190, pred[32,32]{1,0:T(8,128)(4,1)S(1)} %copy-done.15), kind=kOutput, calls=%fused_computation.34 | convolution fusion | flops 17432576 | bytes 2393088 | tf_op jit(solution)/shard_map/scghlm,scmghp->sclghp/dot_general | solution.py:123
  221.5 2.4 fusion.14
  224.0 3.2 %copy.202 = f32[4,16,32,1,2,64]{5,4,2,1,0,3:T(2,128)} copy(f32[4,16,32,1,2,64]{5,2,4,1,0,3:T(8,128)S(1)} %fusion.14) | data formatting | bytes 2097152 | tf_op jit(solution)/shard_map/add | solution.py:145
  227.3 3.6 %reshape.269 = f32[4,512,128]{2,1,0:T(8,128)} reshape(f32[4,16,32,1,2,64]{5,4,2,1,0,3:T(2,128)} %copy.202) | data formatting | bytes 2097152 | tf_op jit(solution)/shard_map/reshape | solution.py:145
  230.8 10.1 %all-gather.2 = bf16[16,1,2,64,128]{4,3,2,1,0:T(8,128)(2,1)S(1)} all-gather(bf16[4,1,2,64,128]{4,3,2,1,0:T(8,128)(2,1)S(1)} %convert_element_type.83), channel_id=4, replica_groups=mesh['sp_0'=4,'sp_1'=4,'tp_0'=4,'tp_1'=2] {'sp_1'}, dimensions={0}, use_global_device_ids=true | all-gather | bytes 655360 | tf_op jit(solution)/shard_map/all_gather | solution.py:67
  241.1 9.9 %all_gather.61 = bf16[4,4,2,64,128]{4,3,2,1,0:T(8,128)(2,1)S(1)} all-gather(bf16[1,4,2,64,128]{4,3,2,1,0:T(8,128)(2,1)S(1)} %bitcast_add_fusion.5), channel_id=1, replica_groups=mesh['sp_0'=4,'sp_1'=4,'tp_0'=4,'tp_1'=2] {'sp_0'}, dimensions={0}, use_global_device_ids=true | all-gather | bytes 655360 | tf_op jit(solution)/shard_map/all_gather | solution.py:67
  257.3 13.1 %all-to-all-start = ((bf16[4,512,128]{2,0,1:T(4,128)(2,1)}), bf16[4,512,128]{2,0,1:T(4,128)(2,1)S(1)}, u32[]{:S(2)}, u32[]{:S(2)}) async-start(bf16[4,512,128]{2,0,1:T(4,128)(2,1)} %copy.223), calls=%async_computation | async-start | bytes 1048576 | tf_op jit(solution)/shard_map/all_to_all | solution.py:258
  271.8 8.0 %all-to-all-done = bf16[4,512,128]{2,0,1:T(4,128)(2,1)S(1)} async-done(((bf16[4,512,128]{2,0,1:T(4,128)(2,1)}), bf16[4,512,128]{2,0,1:T(4,128)(2,1)S(1)}, u32[]{:S(2)}, u32[]{:S(2)}) %all-to-all-start) | async-done | bytes 524320 | tf_op jit(solution)/shard_map/all_to_all | solution.py:258
  279.9 2.7 fusion.24
  (224 shorter events, 101.3 us)
Async XLA Ops:
  6.5 8.0 %copy-start.9 = (bf16[128,64]{0,1:T(8,128)(2,1)S(1)}, bf16[128,64]{0,1:T(8,128)(2,1)}, u32[]{:S(2)}) copy-start(bf16[128,64]{0,1:T(8,128)(2,1)} %param.29) | copy-start | bytes 49156
  6.5 52.9 %all-gather.20.cloned.1.call-start = ((), (), s32[]{:S(2)}) async-start(), calls=%async_computation.4 | async-start | bytes 2236928 | tf_op jit(solution)/shard_map/all_gather | solution.py:30
  11.1 82.0 %all-gather.14.cloned.1.call-start = ((), (), s32[]{:S(2)}) async-start(), calls=%async_computation.1 | async-start | bytes 4718592 | tf_op jit(solution)/shard_map/all_gather | solution.py:39
  12.4 46.4 %copy-start.16 = (f32[4,128]{1,0:T(4,128)S(1)}, f32[4,128]{1,0:T(4,128)}, u32[]{:S(2)}) copy-start(f32[4,128]{1,0:T(4,128)} %param.23) | copy-start | bytes 6148
  12.4 46.4 %copy-start.17 = (f32[4,128]{1,0:T(4,128)S(1)}, f32[4,128]{1,0:T(4,128)}, u32[]{:S(2)}) copy-start(f32[4,128]{1,0:T(4,128)} %param.24) | copy-start | bytes 6148
  12.4 46.4 %copy-start.18 = (f32[4,128]{1,0:T(4,128)S(1)}, f32[4,128]{1,0:T(4,128)}, u32[]{:S(2)}) copy-start(f32[4,128]{1,0:T(4,128)} %param.25) | copy-start | bytes 6148
  14.5 256.0 %all-gather.18.cloned.1.call-start = ((), (), s32[]{:S(2)}) async-start(), calls=%async_computation.3 | async-start | bytes 1572864 | tf_op jit(solution)/shard_map/all_gather | solution.py:91
  47.2 232.7 %all-gather.16.cloned.1.call-start = ((), (), s32[]{:S(2)}) async-start(), calls=%async_computation.2 | async-start | bytes 1310720 | tf_op jit(solution)/shard_map/all_gather | solution.py:91
  106.6 9.9 %copy-start.22 = (f32[2]{0:T(128)S(1)}, f32[2]{0:T(128)}, u32[]{:S(2)}) copy-start(f32[2]{0:T(128)} %param.27) | copy-start | bytes 28
  106.6 9.9 %copy-start.23 = (f32[2]{0:T(128)S(1)}, f32[2]{0:T(128)}, u32[]{:S(2)}) copy-start(f32[2]{0:T(128)} %param.26) | copy-start | bytes 28
  112.7 48.8 %collective-permute-start = (bf16[4,3,384]{2,1,0:T(4,128)(2,1)}, bf16[4,3,384]{2,1,0:T(4,128)(2,1)}, u32[]{:S(2)}, u32[]{:S(2)}) collective-permute-start(bf16[4,3,384]{2,1,0:T(4,128)(2,1)} %copy.233), channel_id=1, source_target_pairs={{0,8},{8,16},{16,24},{24,32},{32,40},{40,48},{48,56},{56,64},{64,7... | collective-permute-start | bytes 27656 | tf_op jit(solution)/shard_map/ppermute | solution.py:53
  145.8 5.1 %copy-start.8 = (f32[4,512,2]{1,2,0:T(2,128)S(1)}, f32[4,512,2]{1,2,0:T(2,128)}, u32[]{:S(2)}) copy-start(f32[4,512,2]{1,2,0:T(2,128)} %get-tuple-element.121) | copy-start | bytes 49156
  147.0 7.0 %copy-start.2 = (f32[4,16,32,2]{3,1,2,0:T(8,128)S(1)}, f32[4,16,32,2]{3,1,2,0:T(8,128)}, u32[]{:S(2)}) copy-start(f32[4,16,32,2]{3,1,2,0:T(8,128)} %get-tuple-element.129) | copy-start | bytes 49156
  176.2 41.6 %copy-start.7 = (f32[4,16,2,32]{3,2,1,0:T(2,128)S(1)}, f32[4,16,2,32]{3,2,1,0:T(2,128)}, u32[]{:S(2)}) copy-start(f32[4,16,2,32]{3,2,1,0:T(2,128)} %copy.194) | copy-start | bytes 49156
  176.2 41.6 %copy-start.15 = (pred[32,32]{1,0:T(8,128)(4,1)S(1)}, pred[32,32]{1,0:T(8,128)(4,1)}, u32[]{:S(2)}) copy-start(pred[32,32]{1,0:T(8,128)(4,1)} %iota_compare_fusion) | copy-start | bytes 3076
  227.2 13.7 %copy-start.19 = (bf16[4,2]{1,0:T(4,128)(2,1)S(1)}, bf16[4,2]{1,0:T(4,128)(2,1)}, u32[]{:S(2)}) copy-start(bf16[4,2]{1,0:T(4,128)(2,1)} %copy.209) | copy-start | bytes 52
  227.2 13.7 %copy-start.20 = (bf16[4,2]{1,0:T(4,128)(2,1)S(1)}, bf16[4,2]{1,0:T(4,128)(2,1)}, u32[]{:S(2)}) copy-start(bf16[4,2]{1,0:T(4,128)(2,1)} %copy.207) | copy-start | bytes 52
  227.2 13.7 %copy-start.21 = (bf16[4,2]{1,0:T(4,128)(2,1)S(1)}, bf16[4,2]{1,0:T(4,128)(2,1)}, u32[]{:S(2)}) copy-start(bf16[4,2]{1,0:T(4,128)(2,1)} %copy.205) | copy-start | bytes 52
  227.2 23.7 %copy-start.25 = (bf16[4,2]{1,0:T(4,128)(2,1)S(1)}, bf16[4,2]{1,0:T(4,128)(2,1)}, u32[]{:S(2)}) copy-start(bf16[4,2]{1,0:T(4,128)(2,1)} %copy.215) | copy-start | bytes 52
  227.2 23.7 %copy-start.26 = (bf16[4,2]{1,0:T(4,128)(2,1)S(1)}, bf16[4,2]{1,0:T(4,128)(2,1)}, u32[]{:S(2)}) copy-start(bf16[4,2]{1,0:T(4,128)(2,1)} %copy.214) | copy-start | bytes 52
  227.2 23.7 %copy-start.27 = (bf16[4,2]{1,0:T(4,128)(2,1)S(1)}, bf16[4,2]{1,0:T(4,128)(2,1)}, u32[]{:S(2)}) copy-start(bf16[4,2]{1,0:T(4,128)(2,1)} %copy.213) | copy-start | bytes 52
  227.2 23.7 %copy-start.28 = (bf16[4,2]{1,0:T(4,128)(2,1)S(1)}, bf16[4,2]{1,0:T(4,128)(2,1)}, u32[]{:S(2)}) copy-start(bf16[4,2]{1,0:T(4,128)(2,1)} %copy.212) | copy-start | bytes 52
  227.3 23.7 %copy-start.29 = (bf16[4,2]{1,0:T(4,128)(2,1)S(1)}, bf16[4,2]{1,0:T(4,128)(2,1)}, u32[]{:S(2)}) copy-start(bf16[4,2]{1,0:T(4,128)(2,1)} %copy.204) | copy-start | bytes 52
  257.3 22.5 %all-to-all-start = ((bf16[4,512,128]{2,0,1:T(4,128)(2,1)}), bf16[4,512,128]{2,0,1:T(4,128)(2,1)S(1)}, u32[]{:S(2)}, u32[]{:S(2)}) async-start(bf16[4,512,128]{2,0,1:T(4,128)(2,1)} %copy.223), calls=%async_computation | async-start | bytes 1048576 | tf_op jit(solution)/shard_map/all_to_all | solution.py:258
  (12 other events, 24.3 us)
Sparse Core Ops, SparseCore 0:
  11.2 46.7 all-gather.19
  59.7 33.3 all-gather.13
  94.8 11.7 all-gather.17
  108.0 22.7 all-gather.15
where the time goes:
time: 291 us; the launch traced here: 289 us
  blocking collectives  78 us (27%)
  local copies, waits for them, and re-layouts  65.5 us (23%)
  other arithmetic  44.6 us (15%)
  waiting for transfers between devices  38.9 us (13%)
  matrix products  31.4 us (11%)
  starting transfers between devices  17 us (6%)
  between operations  13.6 us (5%)
    all_gather x4, blocking collectives, prefix_by_axis(): pieces = jax.tree.map(lambda part: lax.all_gather(part, axis), total)  34.6 us
    all_gather x1, waiting for transfers between devices, over_all(): whole = lax.all_gather(value, axis, axis=dim, tiled=True)  30.8 us
    all_gather x2, blocking collectives, gather_in_order(): parts = lax.all_gather(parts, axes[k])  22 us
    all_gather x2, blocking collectives, gather_axes(): value = lax.all_gather(value, axis, axis=dim, tiled=True)  21.4 us
    while x16, other arithmetic  16.7 us
    dot_general x5, matrix products, project(): jnp.dot(flattened, weight, preferred_element_type=jnp.float32)  13.4 us
    all_to_all x1, starting transfers between devices, local(): lax.all_to_all(gated_all, TP, split_axis=1, concat_axis=2, tiled=True)  13.1 us
    unnamed x73, local copies, waits for them, and re-layouts  12.7 us
  transfers between devices with their start and end apart: 6, of which 2 were waited for; matrix products, arithmetic and copies ran while one was open for 46% of the time, Pallas kernels for 0%

commit v1 on v0

v1 whole, which is shorter than its diff:
```python
import functools

import jax
import jax.numpy as jnp
from jax import lax
from jax.experimental import pallas as pl
from jax.experimental.pallas import tpu as pltpu
from jax.sharding import Mesh
from jax.sharding import PartitionSpec as P

CONV = 4
SP = ("sp_0", "sp_1")
TP = ("tp_0", "tp_1")
SP_TP = ("sp_0", "sp_1", "tp_0", "tp_1")
LENGTH = 8192
SEQS = 4
SPAN = 512
ROWS = 64
WIDTH = 1024
CHUNK = 256
LANES = 128
epsilon = 1e-05
MESH = pl.DeviceIdType.MESH
F32 = jnp.float32
BF16 = jnp.bfloat16


def remote(src, dst, send, recv, device):
    return pltpu.make_async_remote_copy(
        src_ref=src,
        dst_ref=dst,
        send_sem=send,
        recv_sem=recv,
        device_id=device,
        device_id_type=MESH,
    )


class Ring:
    def __init__(self, place, axis, block, sends, recvs, number):
        self.block, self.sends, self.recvs, self.number = block, sends, recvs, number
        self.me = place[axis]
        self.right, self.left = lax.rem(self.me + 1, 4), lax.rem(self.me + 3, 4)
        self.far = lax.rem(self.me + 2, 4)
        to = lambda i: tuple(i if k == axis else p for k, p in enumerate(place))
        self.to_right, self.to_left = to(self.right), to(self.left)

    def copy(self, ref, lane, device):
        return remote(
            ref, ref, self.sends.at[self.number, lane], self.recvs.at[self.number, lane], device
        )

    def own(self):
        self.copy(self.block(self.me, None), 0, self.to_right).start()
        self.copy(self.block(self.me, None), 1, self.to_left).start()

    def near(self):
        self.copy(self.block(self.left, None), 0, self.to_right).wait_recv()
        self.copy(self.block(self.left, 0), 2, self.to_right).start()
        self.copy(self.block(self.right, None), 1, self.to_left).wait_recv()
        self.copy(self.block(self.right, 1), 3, self.to_left).start()

    def last(self):
        self.copy(self.block(self.far, 0), 2, self.to_right).wait_recv()
        self.copy(self.block(self.far, 1), 3, self.to_left).wait_recv()

    def drain(self):
        self.copy(self.block(self.me, None), 0, self.to_right).wait_send()
        self.copy(self.block(self.me, None), 1, self.to_left).wait_send()
        self.copy(self.block(self.left, 0), 2, self.to_right).wait_send()
        self.copy(self.block(self.right, 1), 3, self.to_left).wait_send()


def half_rows(half):
    return slice(None) if half is None else slice(32 * half, 32 * half + 32)


def half_blocks(half):
    return slice(None) if half is None else slice(2 * half, 2 * half + 2)


def matmul(a, b, dims=((1,), (0,)), precision=None):
    return lax.dot_general(a, b, (dims, ((), ())), precision=precision, preferred_element_type=F32)


def silu(value):
    return value / (1.0 + jnp.exp(-value))


def kernel(
    bias_ref,
    rate_ref,
    tokens_ref,
    gain_ref,
    xw_ref,
    zw_ref,
    bw_ref,
    cw_ref,
    dw_ref,
    xt_ref,
    bt_ref,
    ct_ref,
    og_ref,
    ow_ref,
    out_ref,
    T,
    W,
    OT,
    E,
    Z,
    DT,
    CUM,
    XS,
    BS,
    CS,
    Y,
    U,
    SS,
    RS,
    SR,
    RR,
    GT,
    G,
    ring_send,
    ring_recv,
    pair_send,
    pair_recv,
    halo_send,
    halo_recv,
    state_send,
    state_recv,
    back_send,
    back_recv,
    mix_send,
    mix_recv,
    local_sem,
):
    z, y = lax.axis_index("sp_0"), lax.axis_index("sp_1")
    x, c = lax.axis_index("tp_0"), lax.axis_index("tp_1")
    place = (z, y, x, c)
    sp, tp = z * 4 + y, x * 2 + c
    other = 1 - c
    partner = (z, y, x, other)

    def sp_device(i):
        return (i // 4, lax.rem(i, 4), x, c)

    def tp_device(i):
        return (z, y, i // 2, lax.rem(i, 2))

    barrier = pltpu.get_barrier_semaphore()

    def greet_sp(k, _):
        pl.semaphore_signal(
            barrier, inc=1, device_id=sp_device(lax.rem(sp + k, 16)), device_id_type=MESH
        )
        return 0

    def greet_tp(k, _):
        pl.semaphore_signal(
            barrier, inc=1, device_id=tp_device(lax.rem(tp + k, 8)), device_id_type=MESH
        )
        return 0

    lax.fori_loop(1, 16, greet_sp, 0)
    lax.fori_loop(1, 8, greet_tp, 0)

    lane = lax.broadcasted_iota(jnp.int32, (1, LANES), 1)
    low = lane < 64

    W[z, y, :, 0:128] = xw_ref[...]
    W[z, y, :, 128:256] = bw_ref[...]
    W[z, y, :, 256:384] = cw_ref[...]
    W[z, y, :, 384:512] = zw_ref[...]
    dt_columns = dw_ref[...].astype(F32)
    W[z, y, :, 512:640] = jnp.where(low, dt_columns[:, 0:1], dt_columns[:, 1:2]).astype(BF16)

    def normed(s):
        source = tokens_ref[s].astype(F32)
        scale = lax.rsqrt(jnp.mean(source * source, axis=-1, keepdims=True) + epsilon)
        T[s, pl.ds(pl.multiple_of(tp * ROWS, ROWS), ROWS), :] = (
            source * scale * gain_ref[...]
        ).astype(BF16)

    normed(0)
    own_columns = pl.multiple_of((c * 4 + x) * LANES, LANES)
    OT[z, y, :, pl.ds(own_columns, LANES)] = ow_ref[...].astype(F32).T.astype(BF16)
    pl.semaphore_wait(barrier, 22)

    def token_block(s):
        def block(i, half):
            start = (i * 2 + c) * ROWS + (0 if half is None else 32 * half)
            rows = ROWS if half is None else 32
            return T.at[s, pl.ds(pl.multiple_of(start, 32), rows), :]

        return block

    half_start = pl.multiple_of(c * 512, 512)
    cols_a = pl.ds(half_start, 256)
    cols_b = pl.ds(pl.multiple_of(half_start + 256, 256), 256)

    ring = lambda axis, block, number: Ring(place, axis, block, ring_send, ring_recv, number)
    tokens = [ring(2, token_block(s), s) for s in range(SEQS)]
    wa1 = ring(1, lambda i, h: W.at[z, i, half_rows(h), 0:256], 4)
    wb1 = ring(0, lambda i, h: W.at[i, y, half_rows(h), 256:640], 5)
    wa2 = ring(0, lambda i, h: W.at[i, half_blocks(h), :, 0:256], 6)
    wb2 = ring(1, lambda i, h: W.at[half_blocks(h), i, :, 256:640], 7)
    ox = ring(
        2,
        lambda i, h: OT.at[
            z, y, half_rows(h), pl.ds(pl.multiple_of((c * 4 + i) * LANES, LANES), LANES)
        ],
        8,
    )
    oa1 = ring(1, lambda i, h: OT.at[z, i, half_rows(h), cols_a], 9)
    ob1 = ring(0, lambda i, h: OT.at[i, y, half_rows(h), cols_b], 10)
    oa2 = ring(0, lambda i, h: OT.at[i, half_blocks(h), :, cols_a], 11)
    ob2 = ring(1, lambda i, h: OT.at[half_blocks(h), i, :, cols_b], 12)

    def pair_copy(s, k, core):
        i, half = (
            (x, None),
            (tokens[s].left, None),
            (tokens[s].right, None),
            (tokens[s].far, 0),
            (tokens[s].far, 1),
        )[k]
        start = (i * 2 + core) * ROWS + (0 if half is None else 32 * half)
        rows = ROWS if half is None else 32
        ref = T.at[s, pl.ds(pl.multiple_of(start, 32), rows), :]
        return remote(ref, ref, pair_send.at[s, k], pair_recv.at[s, k], partner)

    def out_pair(core):
        ref = OT.at[:, :, :, pl.ds(pl.multiple_of(core * 512, 512), 512)]
        return remote(ref, ref, pair_send.at[SEQS, 0], pair_recv.at[SEQS, 0], partner)

    def token_own(s):
        tokens[s].own()
        pair_copy(s, 0, c).start()

    def token_near(s):
        tokens[s].near()
        pair_copy(s, 1, c).start()
        pair_copy(s, 2, c).start()

    def token_last(s):
        tokens[s].last()
        pair_copy(s, 3, c).start()
        pair_copy(s, 4, c).start()

    token_start = token_own
    wa1.own()
    wb1.own()
    token_start(0)
    normed(1)
    token_start(1)
    ox.own()
    normed(2)
    normed(3)
    wa1.near()
    wb1.near()
    token_near(0)
    token_start(2)
    wa1.last()
    wb1.last()
    wa2.own()
    wb2.own()
    ox.near()
    token_near(1)
    token_start(3)
    wa2.near()
    wb2.near()
    token_last(0)
    ox.last()
    oa1.own()
    ob1.own()
    token_near(2)

    bias = jnp.where(low, bias_ref[0], bias_ref[1])
    rate = jnp.where(low, rate_ref[0], rate_ref[1])
    row_at = lax.broadcasted_iota(jnp.int32, (CHUNK, CHUNK), 0)
    column_at = lax.broadcasted_iota(jnp.int32, (CHUNK, CHUNK), 1)
    lower = row_at >= column_at
    ones_below = lower.astype(F32)
    following = sp_device(lax.rem(sp + 1, 16))

    def halo(s):
        return remote(
            E.at[s, SPAN : SPAN + 8, :],
            E.at[s, 0:8, :],
            halo_send.at[s],
            halo_recv.at[s],
            following,
        )

    def project(s):
        for k in range(5):
            pair_copy(s, k, other).wait_recv()
        weights = W[...].reshape(WIDTH, 640)
        product = matmul(T[s], weights)
        E[s, 8 : SPAN + 8, :] = product[:, 0:384]
        halo(s).start()
        Z[s] = silu(product[:, 384:512])
        step = product[:, 512:640] + bias
        step = jnp.maximum(step, 0.0) + jnp.log1p(jnp.exp(-jnp.abs(step)))
        DT[s] = step
        logdecay = -(step * rate) / LENGTH
        for k in range(2):
            rows = slice(k * CHUNK, (k + 1) * CHUNK)
            CUM[s, rows, :] = matmul(ones_below, logdecay[rows], precision=lax.Precision.HIGHEST)

    def convolve(s):
        halo(s).wait_recv()
        E[s, 0:8, :] = jnp.where(sp == 0, 0.0, E[s, 0:8, :])
        for k, taps_ref in enumerate((xt_ref, bt_ref, ct_ref)):
            columns = slice(k * LANES, (k + 1) * LANES)
            running = taps_ref[0:1, :] * E[s, 5 : 5 + SPAN, columns]
            for offset in range(1, CONV):
                running = (
                    running
                    + taps_ref[offset : offset + 1, :] * E[s, 5 + offset : 5 + offset + SPAN, columns]
                )
            running = silu(running)
            if k == 0:
                XS[s] = (running * DT[s] * jnp.exp(-CUM[s])).astype(BF16)
            elif k == 1:
                BS[s] = running.astype(BF16)
            else:
                CS[s] = running.astype(BF16)

    def states(s):
        for k in range(2):
            rows = slice(k * CHUNK, (k + 1) * CHUNK)
            U[s, k] = matmul(BS[s, rows, :], XS[s, rows, :], ((0,), (0,)))
        first, second = CUM[s, CHUNK - 1 : CHUNK, :], CUM[s, SPAN - 1 : SPAN, :]
        final = jnp.exp(second) * (jnp.exp(first) * U[s, 0] + U[s, 1])
        total = jnp.broadcast_to((first + second).reshape(1, 1, LANES), (16, 8, LANES))
        SS[s] = jnp.concatenate([final.reshape(16, 8, LANES), total], axis=1).astype(BF16)

        def send(k, _):
            i = lax.rem(sp + k, 16)
            remote(
                SS.at[s, i], RS.at[s, sp], state_send.at[s], state_recv.at[s], sp_device(i)
            ).start()
            return 0

        lax.fori_loop(1, 16, send, 0)
        RS[s, sp] = SS[s, sp]

    def inside(s):
        for k in range(2):
            rows = slice(k * CHUNK, (k + 1) * CHUNK)
            scores = matmul(CS[s, rows, :], BS[s, rows, :], ((1,), (1,)))
            scores = jnp.where(lower, scores, 0.0).astype(BF16)
            Y[s, rows, :] = matmul(scores, XS[s, rows, :])

    def scan(s):
        remote(
            SS.at[s, 0:15], RS.at[s, 0:15], state_send.at[s], state_recv.at[s], partner
        ).wait_recv()
        entering = jnp.zeros((8, LANES), F32)
        for i in range(16):
            SR[s, i] = entering
            piece = RS[s, i].astype(F32)
            entering = jnp.exp(piece[8:16]) * entering + piece[0:8]

        def send(k, _):
            i = lax.rem(sp + k, 16)
            remote(
                SR.at[s, i], RR.at[s, sp], back_send.at[s], back_recv.at[s], sp_device(i)
            ).start()
            return 0

        lax.fori_loop(1, 16, send, 0)
        RR[s, sp] = SR[s, sp]

    def finish(s):
        remote(
            SR.at[s, 0:15], RR.at[s, 0:15], back_send.at[s], back_recv.at[s], partner
        ).wait_recv()
        entering = RR[s].reshape(LANES, LANES)
        for k in range(2):
            rows = slice(k * CHUNK, (k + 1) * CHUNK)
            grown = jnp.exp(CUM[s, rows, :])
            whole = grown * (Y[s, rows, :] + matmul(CS[s, rows, :], entering.astype(BF16)))
            if k == 0:
                entering = grown[CHUNK - 1 : CHUNK, :] * (entering + U[s, 0])
            gated = whole * Z[s, rows, :]
            scale = lax.rsqrt(jnp.mean(gated * gated, axis=-1, keepdims=True) + epsilon)
            GT[s, rows, :] = (gated * scale * og_ref[...]).astype(BF16)

        def send(k, _):
            i = lax.rem(tp + k, 8)
            remote(
                GT.at[s, pl.ds(pl.multiple_of(i * ROWS, ROWS), ROWS), :],
                G.at[s, :, pl.ds(own_columns, LANES)],
                mix_send.at[s],
                mix_recv.at[s],
                tp_device(i),
            ).start()
            return 0

        lax.fori_loop(1, 8, send, 0)
        own(s).start()

    def own(s):
        return pltpu.make_async_copy(
            GT.at[s, pl.ds(pl.multiple_of(tp * ROWS, ROWS), ROWS), :],
            G.at[s, :, pl.ds(own_columns, LANES)],
            local_sem.at[s],
        )

    def mixed_in(s):
        remote(
            G.at[s, :, 0:896], G.at[s, :, 0:896], mix_send.at[s], mix_recv.at[s], partner
        ).wait_recv()
        own(s).wait()

    wa2.last()
    wb2.last()
    oa1.near()
    ob1.near()
    token_last(1)
    project(0)
    token_near(3)
    oa1.last()
    ob1.last()
    oa2.own()
    ob2.own()
    convolve(0)
    states(0)
    token_last(2)
    project(1)
    oa2.near()
    ob2.near()
    convolve(1)
    states(1)
    project(2)
    token_last(3)
    convolve(2)
    states(2)
    scan(0)
    inside(0)
    scan(1)
    oa2.last()
    ob2.last()
    out_pair(c).start()
    inside(1)
    project(3)
    finish(0)
    convolve(3)
    states(3)
    scan(2)
    finish(1)
    inside(2)
    inside(3)
    finish(2)
    scan(3)
    out_pair(other).wait_recv()
    finish(3)
    for s in range(SEQS):
        mixed_in(s)
    out_weight = OT[...].reshape(WIDTH, WIDTH)
    result = matmul(G[...].reshape(SEQS * ROWS, WIDTH), out_weight, ((1,), (1,)))
    out_ref[...] = result.astype(BF16).reshape(SEQS, ROWS, WIDTH)

    for each in (*tokens, wa1, wb1, wa2, wb2, ox, oa1, ob1, oa2, ob2):
        each.drain()
    out_pair(c).wait_send()
    for s in range(SEQS):
        for k in range(5):
            pair_copy(s, k, c).wait_send()
        halo(s).wait_send()
        remote(
            SS.at[s, 0:15], RS.at[s, 0:15], state_send.at[s], state_recv.at[s], partner
        ).wait_send()
        remote(
            SR.at[s, 0:15], RR.at[s, 0:15], back_send.at[s], back_recv.at[s], partner
        ).wait_send()
        remote(
            G.at[s, :, 0:896], G.at[s, :, 0:896], mix_send.at[s], mix_recv.at[s], partner
        ).wait_send()


def local(
    tokens,
    norm_gain,
    x_weight,
    z_weight,
    b_weight,
    c_weight,
    dt_weight,
    x_conv,
    b_conv,
    c_conv,
    dt_bias,
    decay_rate,
    out_gain,
    out_weight,
):
    smem = pl.BlockSpec(memory_space=pltpu.SMEM)
    vmem = pl.BlockSpec(memory_space=pltpu.VMEM)
    dma = pltpu.SemaphoreType.DMA
    return pl.pallas_call(
        kernel,
        out_shape=jax.ShapeDtypeStruct(tokens.shape, BF16),
        in_specs=[smem, smem] + [vmem] * 12,
        out_specs=vmem,
        scratch_shapes=[
            pltpu.VMEM((SEQS, SPAN, WIDTH), BF16),
            pltpu.VMEM((4, 4, ROWS, 640), BF16),
            pltpu.VMEM((4, 4, ROWS, WIDTH), BF16),
            pltpu.VMEM((SEQS, SPAN + 8, 384), F32),
            pltpu.VMEM((SEQS, SPAN, LANES), F32),
            pltpu.VMEM((SEQS, SPAN, LANES), F32),
            pltpu.VMEM((SEQS, SPAN, LANES), F32),
            pltpu.VMEM((SEQS, SPAN, LANES), BF16),
            pltpu.VMEM((SEQS, SPAN, LANES), BF16),
            pltpu.VMEM((SEQS, SPAN, LANES), BF16),
            pltpu.VMEM((SEQS, SPAN, LANES), F32),
            pltpu.VMEM((SEQS, 2, LANES, LANES), F32),
            pltpu.VMEM((SEQS, 16, 16, LANES), BF16),
            pltpu.VMEM((SEQS, 16, 16, LANES), BF16),
            pltpu.VMEM((SEQS, 16, 8, LANES), F32),
            pltpu.VMEM((SEQS, 16, 8, LANES), F32),
            pltpu.VMEM((SEQS, SPAN, LANES), BF16),
            pltpu.VMEM((SEQS, ROWS, WIDTH), BF16),
            dma((13, 4)),
            dma((13, 4)),
            dma((SEQS + 1, 5)),
            dma((SEQS + 1, 5)),
            dma((SEQS,)),
            dma((SEQS,)),
            dma((SEQS,)),
            dma((SEQS,)),
            dma((SEQS,)),
            dma((SEQS,)),
            dma((SEQS,)),
            dma((SEQS,)),
            dma((SEQS,)),
        ],
        compiler_params=pltpu.CompilerParams(
            collective_id=0, has_side_effects=True, vmem_limit_bytes=56 * 1024 * 1024
        ),
        name="mixer",
    )(
        dt_bias,
        decay_rate,
        tokens,
        norm_gain.reshape(1, -1),
        x_weight,
        z_weight,
        b_weight,
        c_weight,
        dt_weight,
        x_conv,
        b_conv,
        c_conv,
        out_gain.reshape(1, -1),
        out_weight,
    )


def solution(mesh):
    torus = Mesh(mesh.devices.reshape(4, 4, 4, 2), SP_TP)
    return jax.shard_map(
        local,
        mesh=torus,
        in_specs=(
            P(None, SP_TP, None),
            P(),
            P(SP, TP),
            P(SP, TP),
            P(SP, TP),
            P(SP, TP),
            P(SP, TP),
            P(None, TP),
            P(None, TP),
            P(None, TP),
            P(TP),
            P(TP),
            P(TP),
            P(TP, SP),
        ),
        out_specs=P(None, SP_TP, None),
        check_vma=False,
    )
```

time: 291 us -> 73.5 us (0.25)
  blocking collectives: 78 us -> 0 us
  Pallas kernels: 0 us -> 69.3 us
  local copies, waits for them, and re-layouts: 65.5 us -> 3.96 us
  other arithmetic: 44.6 us -> 0 us
  waiting for transfers between devices: 38.9 us -> 0 us
  matrix products: 31.4 us -> 0 us
  starting transfers between devices: 17 us -> 0 us
  between operations: 13.6 us -> 0.01 us
    all_gather x8 -> x0, blocking collectives: 78 us -> none  [the longest x4 34.6 us: prefix_by_axis(): pieces = jax.tree.map(lambda part: lax.all_gather(part, axis), total)]
    pallas_call x0 -> x1, Pallas kernels: none -> 69.3 us  [local(): pl.pallas_call(kernel, out_shape=jax.ShapeDtypeStruct(tokens.shape, BF16)...]
    dot_general x11 -> x0, matrix products: 31.4 us -> none  [the longest x5 13.4 us: project(): jnp.dot(flattened, weight, preferred_element_type=jnp.float32)]
    all_gather x4 -> x0, waiting for transfers between devices: 30.8 us -> none  [the longest x1 30.8 us: over_all(): whole = lax.all_gather(value, axis, axis=dim, tiled=True)]
    while x16 -> x0, other arithmetic: 16.7 us -> none
    mul x39 -> x0, local copies, waits for them, and re-layouts: 16.3 us -> none  [the longest x32 12.1 us: advance(): running_state * shrink[..., None, None] + fresh_state]
    reshape x8 -> x0, local copies, waits for them, and re-layouts: 16 us -> none  [the longest x1 4.99 us: project(): jnp.concatenate(pieces_out, axis=1)]
    all_to_all x1 -> x0, starting transfers between devices: 13.1 us -> none  [local(): lax.all_to_all(gated_all, TP, split_axis=1, concat_axis=2, tiled=True)]
  transfers between devices with their start and end apart: 6 -> 0, of which waited for: 2 -> 0; matrix products, arithmetic and copies ran while one was open for 46% -> 0% of each run, Pallas kernels for 0% -> 0%
where the time goes in v1:
time: 73.5 us; the launch traced here: 73.3 us
  Pallas kernels  69.3 us (94%)
  local copies, waits for them, and re-layouts  3.96 us (5%)
    pallas_call x1, Pallas kernels, local(): pl.pallas_call(kernel, out_shape=jax.ShapeDtypeStruct(tokens.shape, BF16)...  69.3 us
    unnamed x5, local copies, waits for them, and re-layouts  3.96 us

profile of v1, /device:TPU:1, one launch (start us, length us, event | category | flops | bytes accessed | tf_op | source)
XLA Modules:
  0.0 73.3 jit_solution(14405473438894810888)
XLA Ops:
  0.0 0.0 copy-start
  0.0 1.4 %copy.15.dw_ref = bf16[64,2]{1,0:T(8,128)(2,1)} copy(bf16[64,2]{0,1:T(2,128)(2,1)} %param.20) | data formatting | bytes 512 | tf_op args[6]
  1.4 0.0 copy-done
  1.4 0.7 copy.16.ow_ref
  2.1 69.3 %mixer.1 = bf16[4,64,1024]{2,1,0:T(8,128)(2,1)} custom-call(f32[2]{0:T(128)} %bias_ref.1, f32[2]{0:T(128)} %rate_ref.1, bf16[4,64,1024]{2,1,0:T(8,128)(2,1)} %tokens_ref.1, f32[1,1024]{1,0:T(1,128)} %bitcast.2, bf16[64,128]{1,0:T(8,128)(2,1)} %xw_ref.1, bf16[64,128]{1,0:T(8,128)(2,1)} %zw_ref.1, bf16[64,128]{1,0:T(8,128)(2,1)} %bw_ref.1, ...), custom_call_target="tpu_custom_call" | custom-call | tf_op jit(solution)/shard_map/mixer/pallas_call | solution.py:504
  71.4 1.9 %copy.18 = bf16[4,64,1024]{2,1,0:T(8,128)(2,1)} copy(bf16[4,64,1024]{2,1,0:T(8,128)(2,1)} %mixer.1) | data formatting | bytes 1048576
Async XLA Ops:
  0.0 1.4 %copy-start = (bf16[128,64]{0,1:T(8,128)(2,1)S(1)}, bf16[128,64]{0,1:T(8,128)(2,1)}, u32[]{:S(2)}) copy-start(bf16[128,64]{0,1:T(8,128)(2,1)} %param.27) | copy-start | bytes 49156

commit v2 on v1

--- a/solution.py
+++ b/solution.py
@@ -84,7 +84,8 @@
 
 
 def silu(value):
-    return value / (1.0 + jnp.exp(-value))
+    half = 0.5 * value
+    return half + half * jnp.tanh(half)
 
 
 def kernel(
@@ -149,21 +150,11 @@
         return (z, y, i // 2, lax.rem(i, 2))
 
     barrier = pltpu.get_barrier_semaphore()
-
-    def greet_sp(k, _):
-        pl.semaphore_signal(
-            barrier, inc=1, device_id=sp_device(lax.rem(sp + k, 16)), device_id_type=MESH
-        )
-        return 0
-
-    def greet_tp(k, _):
-        pl.semaphore_signal(
-            barrier, inc=1, device_id=tp_device(lax.rem(tp + k, 8)), device_id_type=MESH
-        )
-        return 0
-
-    lax.fori_loop(1, 16, greet_sp, 0)
-    lax.fori_loop(1, 8, greet_tp, 0)
+    for step in (1, 3):
+        for axis in range(3):
+            near = tuple(lax.rem(p + step, 4) if k == axis else p for k, p in enumerate(place))
+            pl.semaphore_signal(barrier, inc=1, device_id=near, device_id_type=MESH)
+    pl.semaphore_signal(barrier, inc=1, device_id=partner, device_id_type=MESH)
 
     lane = lax.broadcasted_iota(jnp.int32, (1, LANES), 1)
     low = lane < 64
@@ -172,8 +163,10 @@
     W[z, y, :, 128:256] = bw_ref[...]
     W[z, y, :, 256:384] = cw_ref[...]
     W[z, y, :, 384:512] = zw_ref[...]
-    dt_columns = dw_ref[...].astype(F32)
-    W[z, y, :, 512:640] = jnp.where(low, dt_columns[:, 0:1], dt_columns[:, 1:2]).astype(BF16)
+    head_at = lax.broadcasted_iota(jnp.int32, (2, LANES), 0)
+    lane_at = lax.broadcasted_iota(jnp.int32, (2, LANES), 1)
+    spread = (lane_at // 64 == head_at).astype(BF16)
+    W[z, y, :, 512:640] = matmul(dw_ref[...], spread, ((0,), (0,))).astype(BF16)
 
     def normed(s):
         source = tokens_ref[s].astype(F32)
@@ -184,8 +177,8 @@
 
     normed(0)
     own_columns = pl.multiple_of((c * 4 + x) * LANES, LANES)
-    OT[z, y, :, pl.ds(own_columns, LANES)] = ow_ref[...].astype(F32).T.astype(BF16)
-    pl.semaphore_wait(barrier, 22)
+    OT[z, y, :, pl.ds(own_columns, LANES)] = ow_ref[...]
+    pl.semaphore_wait(barrier, 7)
 
     def token_block(s):
         def block(i, half):
@@ -248,46 +241,47 @@
         pair_copy(s, 3, c).start()
         pair_copy(s, 4, c).start()
 
-    token_start = token_own
     wa1.own()
     wb1.own()
-    token_start(0)
+    ox.own()
+    token_own(0)
     normed(1)
-    token_start(1)
-    ox.own()
+    token_own(1)
     normed(2)
     normed(3)
     wa1.near()
     wb1.near()
+    wa1.last()
+    wa2.own()
+    wb1.last()
+    wb2.own()
     token_near(0)
-    token_start(2)
-    wa1.last()
-    wb1.last()
-    wa2.own()
-    wb2.own()
+    token_own(2)
     ox.near()
-    token_near(1)
-    token_start(3)
     wa2.near()
     wb2.near()
+    token_near(1)
+    token_own(3)
     token_last(0)
     ox.last()
     oa1.own()
     ob1.own()
-    token_near(2)
+    wa2.last()
+    wb2.last()
 
     bias = jnp.where(low, bias_ref[0], bias_ref[1])
     rate = jnp.where(low, rate_ref[0], rate_ref[1])
     row_at = lax.broadcasted_iota(jnp.int32, (CHUNK, CHUNK), 0)
     column_at = lax.broadcasted_iota(jnp.int32, (CHUNK, CHUNK), 1)
     lower = row_at >= column_at
-    ones_below = lower.astype(F32)
+    ones_below = lower.astype(BF16)
+    tiles = [slice(k * ROWS, (k + 1) * ROWS) for k in range(SPAN // ROWS)]
     following = sp_device(lax.rem(sp + 1, 16))
 
     def halo(s):
         return remote(
-            E.at[s, SPAN : SPAN + 8, :],
-            E.at[s, 0:8, :],
+            E.at[s, :, SPAN : SPAN + 8, :],
+            E.at[s, :, 0:8, :],
             halo_send.at[s],
             halo_recv.at[s],
             following,
@@ -298,35 +292,41 @@
             pair_copy(s, k, other).wait_recv()
         weights = W[...].reshape(WIDTH, 640)
         product = matmul(T[s], weights)
-        E[s, 8 : SPAN + 8, :] = product[:, 0:384]
+        for k in range(3):
+            E[s, k, 8 : SPAN + 8, :] = product[:, k * LANES : (k + 1) * LANES]
+        Z[s] = product[:, 384:512]
+        DT[s] = product[:, 512:640]
         halo(s).start()
-        Z[s] = silu(product[:, 384:512])
-        step = product[:, 512:640] + bias
-        step = jnp.maximum(step, 0.0) + jnp.log1p(jnp.exp(-jnp.abs(step)))
-        DT[s] = step
-        logdecay = -(step * rate) / LENGTH
+        for rows in tiles:
+            Z[s, rows, :] = silu(Z[s, rows, :])
+            step = DT[s, rows, :] + bias
+            step = jnp.maximum(step, 0.0) + jnp.log1p(jnp.exp(-jnp.abs(step)))
+            DT[s, rows, :] = step
+            XS[s, rows, :] = (-(step * rate) / LENGTH).astype(BF16)
         for k in range(2):
             rows = slice(k * CHUNK, (k + 1) * CHUNK)
-            CUM[s, rows, :] = matmul(ones_below, logdecay[rows], precision=lax.Precision.HIGHEST)
+            CUM[s, rows, :] = matmul(ones_below, XS[s, rows, :])
 
     def convolve(s):
         halo(s).wait_recv()
-        E[s, 0:8, :] = jnp.where(sp == 0, 0.0, E[s, 0:8, :])
+        for k in range(3):
+            E[s, k, 0:8, :] = jnp.where(sp == 0, 0.0, E[s, k, 0:8, :])
         for k, taps_ref in enumerate((xt_ref, bt_ref, ct_ref)):
-            columns = slice(k * LANES, (k + 1) * LANES)
-            running = taps_ref[0:1, :] * E[s, 5 : 5 + SPAN, columns]
-            for offset in range(1, CONV):
-                running = (
-                    running
-                    + taps_ref[offset : offset + 1, :] * E[s, 5 + offset : 5 + offset + SPAN, columns]
-                )
-            running = silu(running)
-            if k == 0:
-                XS[s] = (running * DT[s] * jnp.exp(-CUM[s])).astype(BF16)
-            elif k == 1:
-                BS[s] = running.astype(BF16)
-            else:
-                CS[s] = running.astype(BF16)
+            taps = [taps_ref[offset : offset + 1, :] for offset in range(CONV)]
+            for rows in tiles:
+                start = rows.start + 5
+                running = taps[0] * E[s, k, start : start + ROWS, :]
+                for offset in range(1, CONV):
+                    first = start + offset
+                    running = running + taps[offset] * E[s, k, first : first + ROWS, :]
+                running = silu(running)
+                if k == 0:
+                    decayed = DT[s, rows, :] * jnp.exp(-CUM[s, rows, :])
+                    XS[s, rows, :] = (running * decayed).astype(BF16)
+                elif k == 1:
+                    BS[s, rows, :] = running.astype(BF16)
+                else:
+                    CS[s, rows, :] = running.astype(BF16)
 
     def states(s):
         for k in range(2):
@@ -381,11 +381,12 @@
         entering = RR[s].reshape(LANES, LANES)
         for k in range(2):
             rows = slice(k * CHUNK, (k + 1) * CHUNK)
-            grown = jnp.exp(CUM[s, rows, :])
-            whole = grown * (Y[s, rows, :] + matmul(CS[s, rows, :], entering.astype(BF16)))
+            Y[s, rows, :] += matmul(CS[s, rows, :], entering.astype(BF16))
             if k == 0:
-                entering = grown[CHUNK - 1 : CHUNK, :] * (entering + U[s, 0])
-            gated = whole * Z[s, rows, :]
+                grown = jnp.exp(CUM[s, CHUNK - 1 : CHUNK, :])
+                entering = grown * (entering + U[s, 0])
+        for rows in tiles:
+            gated = Y[s, rows, :] * jnp.exp(CUM[s, rows, :]) * Z[s, rows, :]
             scale = lax.rsqrt(jnp.mean(gated * gated, axis=-1, keepdims=True) + epsilon)
             GT[s, rows, :] = (gated * scale * og_ref[...]).astype(BF16)
 
@@ -416,53 +417,56 @@
         ).wait_recv()
         own(s).wait()
 
-    wa2.last()
-    wb2.last()
+    def multiply(first, last):
+        for s in range(first, last):
+            mixed_in(s)
+        gathered = G[first:last].reshape((last - first) * ROWS, WIDTH)
+        result = matmul(gathered, OT[...].reshape(WIDTH, WIDTH), ((1,), (1,)))
+        out_ref[first:last] = result.astype(BF16).reshape(last - first, ROWS, WIDTH)
+
+    project(0)
+    token_near(2)
     oa1.near()
     ob1.near()
     token_last(1)
-    project(0)
-    token_near(3)
+    project(1)
+    convolve(0)
+    states(0)
     oa1.last()
     ob1.last()
     oa2.own()
     ob2.own()
-    convolve(0)
-    states(0)
+    token_near(3)
+    convolve(1)
+    states(1)
     token_last(2)
-    project(1)
+    inside(0)
+    project(2)
+    scan(0)
     oa2.near()
     ob2.near()
-    convolve(1)
-    states(1)
-    project(2)
+    inside(1)
+    scan(1)
     token_last(3)
+    project(3)
     convolve(2)
     states(2)
-    scan(0)
-    inside(0)
-    scan(1)
+    finish(0)
+    convolve(3)
+    states(3)
     oa2.last()
     ob2.last()
     out_pair(c).start()
-    inside(1)
-    project(3)
-    finish(0)
-    convolve(3)
-    states(3)
     scan(2)
     finish(1)
     inside(2)
+    scan(3)
     inside(3)
     finish(2)
-    scan(3)
     out_pair(other).wait_recv()
+    multiply(0, 3)
     finish(3)
-    for s in range(SEQS):
-        mixed_in(s)
-    out_weight = OT[...].reshape(WIDTH, WIDTH)
-    result = matmul(G[...].reshape(SEQS * ROWS, WIDTH), out_weight, ((1,), (1,)))
-    out_ref[...] = result.astype(BF16).reshape(SEQS, ROWS, WIDTH)
+    multiply(3, 4)
 
     for each in (*tokens, wa1, wb1, wa2, wb2, ox, oa1, ob1, oa2, ob2):
         each.drain()
@@ -510,7 +514,7 @@
             pltpu.VMEM((SEQS, SPAN, WIDTH), BF16),
             pltpu.VMEM((4, 4, ROWS, 640), BF16),
             pltpu.VMEM((4, 4, ROWS, WIDTH), BF16),
-            pltpu.VMEM((SEQS, SPAN + 8, 384), F32),
+            pltpu.VMEM((SEQS, 3, SPAN + 8, LANES), F32),
             pltpu.VMEM((SEQS, SPAN, LANES), F32),
             pltpu.VMEM((SEQS, SPAN, LANES), F32),
             pltpu.VMEM((SEQS, SPAN, LANES), F32),
@@ -552,12 +556,12 @@
         z_weight,
         b_weight,
         c_weight,
-        dt_weight,
+        dt_weight.T,
         x_conv,
         b_conv,
         c_conv,
         out_gain.reshape(1, -1),
-        out_weight,
+        out_weight.T,
     )
 
 

time: 73.5 us -> 66.2 us (0.901)
  Pallas kernels: 69.3 us -> 64.2 us
  local copies, waits for them, and re-layouts: 3.96 us -> 1.87 us
    pallas_call x1, Pallas kernels: 69.3 us -> 64.2 us  [local(): pl.pallas_call(kernel, out_shape=jax.ShapeDtypeStruct(tokens.shape, BF16)...]
    unnamed x5 -> x1, local copies, waits for them, and re-layouts: 3.96 us -> 1.87 us
where the time goes in v2:
time: 66.2 us; the launch traced here: 66 us
  Pallas kernels  64.2 us (97%)
  local copies, waits for them, and re-layouts  1.87 us (3%)
    pallas_call x1, Pallas kernels, local(): pl.pallas_call(kernel, out_shape=jax.ShapeDtypeStruct(tokens.shape, BF16)...  64.2 us
    unnamed x1, local copies, waits for them, and re-layouts  1.87 us

profile of v2, /device:TPU:1, one launch (start us, length us, event | category | flops | bytes accessed | tf_op | source)
XLA Modules:
  0.0 66.0 jit_solution(8252551945296029803)
XLA Ops:
  0.0 64.2 %mixer.1 = bf16[4,64,1024]{2,1,0:T(8,128)(2,1)} custom-call(f32[2]{0:T(128)} %bias_ref.1, f32[2]{0:T(128)} %rate_ref.1, bf16[4,64,1024]{2,1,0:T(8,128)(2,1)} %tokens_ref.1, f32[1,1024]{1,0:T(1,128)} %bitcast.5, bf16[64,128]{1,0:T(8,128)(2,1)} %xw_ref.1, bf16[64,128]{1,0:T(8,128)(2,1)} %zw_ref.1, bf16[64,128]{1,0:T(8,128)(2,1)} %bw_ref.1, ...), custom_call_target="tpu_custom_call" | custom-call | tf_op jit(solution)/shard_map/mixer/pallas_call | solution.py:508
  64.2 1.9 %copy.16 = bf16[4,64,1024]{2,1,0:T(8,128)(2,1)} copy(bf16[4,64,1024]{2,1,0:T(8,128)(2,1)} %mixer.1) | data formatting | bytes 1048576

commit v3 on v2

--- a/solution.py
+++ b/solution.py
@@ -105,8 +105,10 @@
     ow_ref,
     out_ref,
     T,
-    W,
-    OT,
+    WA,
+    WB,
+    OY,
+    O,
     E,
     Z,
     DT,
@@ -159,14 +161,14 @@
     lane = lax.broadcasted_iota(jnp.int32, (1, LANES), 1)
     low = lane < 64
 
-    W[z, y, :, 0:128] = xw_ref[...]
-    W[z, y, :, 128:256] = bw_ref[...]
-    W[z, y, :, 256:384] = cw_ref[...]
-    W[z, y, :, 384:512] = zw_ref[...]
+    WA[z, y, :, 0:128] = xw_ref[...]
+    WA[z, y, :, 128:256] = bw_ref[...]
+    WB[z, y, :, 0:128] = cw_ref[...]
+    WB[z, y, :, 128:256] = zw_ref[...]
     head_at = lax.broadcasted_iota(jnp.int32, (2, LANES), 0)
     lane_at = lax.broadcasted_iota(jnp.int32, (2, LANES), 1)
     spread = (lane_at // 64 == head_at).astype(BF16)
-    W[z, y, :, 512:640] = matmul(dw_ref[...], spread, ((0,), (0,))).astype(BF16)
+    WB[z, y, :, 256:384] = matmul(dw_ref[...], spread, ((0,), (0,))).astype(BF16)
 
     def normed(s):
         source = tokens_ref[s].astype(F32)
@@ -177,7 +179,7 @@
 
     normed(0)
     own_columns = pl.multiple_of((c * 4 + x) * LANES, LANES)
-    OT[z, y, :, pl.ds(own_columns, LANES)] = ow_ref[...]
+    OY[y, :, pl.ds(pl.multiple_of(x * LANES, LANES), LANES)] = ow_ref[...]
     pl.semaphore_wait(barrier, 7)
 
     def token_block(s):
@@ -188,27 +190,28 @@
 
         return block
 
-    half_start = pl.multiple_of(c * 512, 512)
-    cols_a = pl.ds(half_start, 256)
-    cols_b = pl.ds(pl.multiple_of(half_start + 256, 256), 256)
-
     ring = lambda axis, block, number: Ring(place, axis, block, ring_send, ring_recv, number)
     tokens = [ring(2, token_block(s), s) for s in range(SEQS)]
-    wa1 = ring(1, lambda i, h: W.at[z, i, half_rows(h), 0:256], 4)
-    wb1 = ring(0, lambda i, h: W.at[i, y, half_rows(h), 256:640], 5)
-    wa2 = ring(0, lambda i, h: W.at[i, half_blocks(h), :, 0:256], 6)
-    wb2 = ring(1, lambda i, h: W.at[half_blocks(h), i, :, 256:640], 7)
+    wa1 = ring(1, lambda i, h: WA.at[z, i, half_rows(h)], 4)
+    wb1 = ring(0, lambda i, h: WB.at[i, y, half_rows(h)], 5)
+    shifted = lambda i, k: lax.rem(i + k, 4)
+    wa2 = [ring(0, lambda i, h, k=k: WA.at[i, shifted(y, k), half_rows(h)], 6 + k) for k in range(4)]
+    wb2 = [ring(1, lambda i, h, k=k: WB.at[shifted(z, k), i, half_rows(h)], 10 + k) for k in range(4)]
     ox = ring(
         2,
-        lambda i, h: OT.at[
-            z, y, half_rows(h), pl.ds(pl.multiple_of((c * 4 + i) * LANES, LANES), LANES)
+        lambda i, h: OY.at[y, half_rows(h), pl.ds(pl.multiple_of(i * LANES, LANES), LANES)],
+        14,
+    )
+    oy = ring(1, lambda i, h: OY.at[i, half_rows(h)], 15)
+    oz = ring(
+        0,
+        lambda i, h: O.at[
+            c,
+            slice(None) if h is None else slice(256 * h, 256 * h + 256),
+            pl.ds(pl.multiple_of(i * 256, 256), 256),
         ],
-        8,
+        16,
     )
-    oa1 = ring(1, lambda i, h: OT.at[z, i, half_rows(h), cols_a], 9)
-    ob1 = ring(0, lambda i, h: OT.at[i, y, half_rows(h), cols_b], 10)
-    oa2 = ring(0, lambda i, h: OT.at[i, half_blocks(h), :, cols_a], 11)
-    ob2 = ring(1, lambda i, h: OT.at[half_blocks(h), i, :, cols_b], 12)
 
     def pair_copy(s, k, core):
         i, half = (
@@ -224,7 +227,7 @@
         return remote(ref, ref, pair_send.at[s, k], pair_recv.at[s, k], partner)
 
     def out_pair(core):
-        ref = OT.at[:, :, :, pl.ds(pl.multiple_of(core * 512, 512), 512)]
+        ref = O.at[core]
         return remote(ref, ref, pair_send.at[SEQS, 0], pair_recv.at[SEQS, 0], partner)
 
     def token_own(s):
@@ -243,6 +246,8 @@
 
     wa1.own()
     wb1.own()
+    wa2[0].own()
+    wb2[0].own()
     ox.own()
     token_own(0)
     normed(1)
@@ -250,24 +255,40 @@
     normed(2)
     normed(3)
     wa1.near()
+    wa2[1].own()
+    wa2[3].own()
     wb1.near()
-    wa1.last()
-    wa2.own()
-    wb1.last()
-    wb2.own()
+    wb2[1].own()
+    wb2[3].own()
+    wa2[0].near()
+    wb2[0].near()
+    ox.near()
     token_near(0)
     token_own(2)
-    ox.near()
-    wa2.near()
-    wb2.near()
+    wa1.last()
+    wa2[2].own()
+    wb1.last()
+    wb2[2].own()
+    wa2[1].near()
+    wa2[3].near()
+    wb2[1].near()
+    wb2[3].near()
+    ox.last()
+    oy.own()
+    wa2[2].near()
+    wb2[2].near()
+    token_last(0)
     token_near(1)
     token_own(3)
-    token_last(0)
-    ox.last()
-    oa1.own()
-    ob1.own()
-    wa2.last()
-    wb2.last()
+    oy.near()
+    wa2[0].last()
+    wa2[1].last()
+    wa2[3].last()
+    wa2[2].last()
+    wb2[0].last()
+    wb2[1].last()
+    wb2[3].last()
+    wb2[2].last()
 
     bias = jnp.where(low, bias_ref[0], bias_ref[1])
     rate = jnp.where(low, rate_ref[0], rate_ref[1])
@@ -290,12 +311,13 @@
     def project(s):
         for k in range(5):
             pair_copy(s, k, other).wait_recv()
-        weights = W[...].reshape(WIDTH, 640)
-        product = matmul(T[s], weights)
-        for k in range(3):
-            E[s, k, 8 : SPAN + 8, :] = product[:, k * LANES : (k + 1) * LANES]
-        Z[s] = product[:, 384:512]
-        DT[s] = product[:, 512:640]
+        product = matmul(T[s], WA[...].reshape(WIDTH, 256))
+        E[s, 0, 8 : SPAN + 8, :] = product[:, 0:128]
+        E[s, 1, 8 : SPAN + 8, :] = product[:, 128:256]
+        product = matmul(T[s], WB[...].reshape(WIDTH, 384))
+        E[s, 2, 8 : SPAN + 8, :] = product[:, 0:128]
+        Z[s] = product[:, 128:256]
+        DT[s] = product[:, 256:384]
         halo(s).start()
         for rows in tiles:
             Z[s, rows, :] = silu(Z[s, rows, :])
@@ -421,54 +443,53 @@
         for s in range(first, last):
             mixed_in(s)
         gathered = G[first:last].reshape((last - first) * ROWS, WIDTH)
-        result = matmul(gathered, OT[...].reshape(WIDTH, WIDTH), ((1,), (1,)))
+        result = matmul(gathered, O[...].reshape(WIDTH, WIDTH))
         out_ref[first:last] = result.astype(BF16).reshape(last - first, ROWS, WIDTH)
+
+    def turn():
+        block = OY[...].reshape(256, 512).astype(F32).T.astype(BF16)
+        O[c, :, pl.ds(pl.multiple_of(z * 256, 256), 256)] = block
 
     project(0)
     token_near(2)
-    oa1.near()
-    ob1.near()
+    oy.last()
+    turn()
+    oz.own()
     token_last(1)
     project(1)
     convolve(0)
     states(0)
-    oa1.last()
-    ob1.last()
-    oa2.own()
-    ob2.own()
     token_near(3)
+    oz.near()
     convolve(1)
     states(1)
+    inside(0)
     token_last(2)
-    inside(0)
     project(2)
     scan(0)
-    oa2.near()
-    ob2.near()
     inside(1)
     scan(1)
+    convolve(2)
+    states(2)
+    oz.last()
+    out_pair(c).start()
     token_last(3)
     project(3)
-    convolve(2)
-    states(2)
     finish(0)
+    finish(1)
     convolve(3)
     states(3)
-    oa2.last()
-    ob2.last()
-    out_pair(c).start()
     scan(2)
-    finish(1)
     inside(2)
-    scan(3)
     inside(3)
     finish(2)
+    scan(3)
     out_pair(other).wait_recv()
     multiply(0, 3)
     finish(3)
     multiply(3, 4)
 
-    for each in (*tokens, wa1, wb1, wa2, wb2, ox, oa1, ob1, oa2, ob2):
+    for each in (*tokens, wa1, wb1, *wa2, *wb2, ox, oy, oz):
         each.drain()
     out_pair(c).wait_send()
     for s in range(SEQS):
@@ -512,8 +533,10 @@
         out_specs=vmem,
         scratch_shapes=[
             pltpu.VMEM((SEQS, SPAN, WIDTH), BF16),
-            pltpu.VMEM((4, 4, ROWS, 640), BF16),
-            pltpu.VMEM((4, 4, ROWS, WIDTH), BF16),
+            pltpu.VMEM((4, 4, ROWS, 256), BF16),
+            pltpu.VMEM((4, 4, ROWS, 384), BF16),
+            pltpu.VMEM((4, ROWS, 512), BF16),
+            pltpu.VMEM((2, 512, WIDTH), BF16),
             pltpu.VMEM((SEQS, 3, SPAN + 8, LANES), F32),
             pltpu.VMEM((SEQS, SPAN, LANES), F32),
             pltpu.VMEM((SEQS, SPAN, LANES), F32),
@@ -529,8 +552,8 @@
             pltpu.VMEM((SEQS, 16, 8, LANES), F32),
             pltpu.VMEM((SEQS, SPAN, LANES), BF16),
             pltpu.VMEM((SEQS, ROWS, WIDTH), BF16),
-            dma((13, 4)),
-            dma((13, 4)),
+            dma((17, 4)),
+            dma((17, 4)),
             dma((SEQS + 1, 5)),
             dma((SEQS + 1, 5)),
             dma((SEQS,)),

time: 66.2 us -> 67.9 us (1.026)
  Pallas kernels: 64.2 us -> 65.8 us
    pallas_call x1, Pallas kernels: 64.2 us -> 65.8 us  [local(): pl.pallas_call(kernel, out_shape=jax.ShapeDtypeStruct(tokens.shape, BF16)...]
where the time goes in v3:
time: 67.9 us; the launch traced here: 67.7 us
  Pallas kernels  65.8 us (97%)
  local copies, waits for them, and re-layouts  1.87 us (3%)
    pallas_call x1, Pallas kernels, local(): pl.pallas_call(kernel, out_shape=jax.ShapeDtypeStruct(tokens.shape, BF16)...  65.8 us
    unnamed x1, local copies, waits for them, and re-layouts  1.87 us

profile of v3, /device:TPU:1, one launch (start us, length us, event | category | flops | bytes accessed | tf_op | source)
XLA Modules:
  0.0 67.7 jit_solution(139580260411272206)
XLA Ops:
  0.0 65.8 %mixer.1 = bf16[4,64,1024]{2,1,0:T(8,128)(2,1)} custom-call(f32[2]{0:T(128)} %bias_ref.1, f32[2]{0:T(128)} %rate_ref.1, bf16[4,64,1024]{2,1,0:T(8,128)(2,1)} %tokens_ref.1, f32[1,1024]{1,0:T(1,128)} %bitcast.5, bf16[64,128]{1,0:T(8,128)(2,1)} %xw_ref.1, bf16[64,128]{1,0:T(8,128)(2,1)} %zw_ref.1, bf16[64,128]{1,0:T(8,128)(2,1)} %bw_ref.1, ...), custom_call_target="tpu_custom_call" | custom-call | tf_op jit(solution)/shard_map/mixer/pallas_call | solution.py:529
  65.8 1.9 %copy.16 = bf16[4,64,1024]{2,1,0:T(8,128)(2,1)} copy(bf16[4,64,1024]{2,1,0:T(8,128)(2,1)} %mixer.1) | data formatting | bytes 1048576

commit v4 on v3

--- a/solution.py
+++ b/solution.py
@@ -37,13 +37,14 @@
 
 
 class Ring:
-    def __init__(self, place, axis, block, sends, recvs, number):
+    def __init__(self, place, axis, block, sends, recvs, number, direct=False):
         self.block, self.sends, self.recvs, self.number = block, sends, recvs, number
+        self.direct = direct
         self.me = place[axis]
         self.right, self.left = lax.rem(self.me + 1, 4), lax.rem(self.me + 3, 4)
         self.far = lax.rem(self.me + 2, 4)
         to = lambda i: tuple(i if k == axis else p for k, p in enumerate(place))
-        self.to_right, self.to_left = to(self.right), to(self.left)
+        self.to_right, self.to_left, self.to_far = to(self.right), to(self.left), to(self.far)
 
     def copy(self, ref, lane, device):
         return remote(
@@ -53,22 +54,32 @@
     def own(self):
         self.copy(self.block(self.me, None), 0, self.to_right).start()
         self.copy(self.block(self.me, None), 1, self.to_left).start()
+        if self.direct:
+            self.copy(self.block(self.me, None), 2, self.to_far).start()
 
     def near(self):
         self.copy(self.block(self.left, None), 0, self.to_right).wait_recv()
-        self.copy(self.block(self.left, 0), 2, self.to_right).start()
+        if not self.direct:
+            self.copy(self.block(self.left, 0), 2, self.to_right).start()
         self.copy(self.block(self.right, None), 1, self.to_left).wait_recv()
-        self.copy(self.block(self.right, 1), 3, self.to_left).start()
+        if not self.direct:
+            self.copy(self.block(self.right, 1), 3, self.to_left).start()
 
     def last(self):
-        self.copy(self.block(self.far, 0), 2, self.to_right).wait_recv()
-        self.copy(self.block(self.far, 1), 3, self.to_left).wait_recv()
+        if self.direct:
+            self.copy(self.block(self.far, None), 2, self.to_far).wait_recv()
+        else:
+            self.copy(self.block(self.far, 0), 2, self.to_right).wait_recv()
+            self.copy(self.block(self.far, 1), 3, self.to_left).wait_recv()
 
     def drain(self):
         self.copy(self.block(self.me, None), 0, self.to_right).wait_send()
         self.copy(self.block(self.me, None), 1, self.to_left).wait_send()
-        self.copy(self.block(self.left, 0), 2, self.to_right).wait_send()
-        self.copy(self.block(self.right, 1), 3, self.to_left).wait_send()
+        if self.direct:
+            self.copy(self.block(self.me, None), 2, self.to_far).wait_send()
+        else:
+            self.copy(self.block(self.left, 0), 2, self.to_right).wait_send()
+            self.copy(self.block(self.right, 1), 3, self.to_left).wait_send()
 
 
 def half_rows(half):
@@ -152,7 +163,7 @@
         return (z, y, i // 2, lax.rem(i, 2))
 
     barrier = pltpu.get_barrier_semaphore()
-    for step in (1, 3):
+    for step in (1, 2, 3):
         for axis in range(3):
             near = tuple(lax.rem(p + step, 4) if k == axis else p for k, p in enumerate(place))
             pl.semaphore_signal(barrier, inc=1, device_id=near, device_id_type=MESH)
@@ -180,7 +191,7 @@
     normed(0)
     own_columns = pl.multiple_of((c * 4 + x) * LANES, LANES)
     OY[y, :, pl.ds(pl.multiple_of(x * LANES, LANES), LANES)] = ow_ref[...]
-    pl.semaphore_wait(barrier, 7)
+    pl.semaphore_wait(barrier, 10)
 
     def token_block(s):
         def block(i, half):
@@ -190,10 +201,12 @@
 
         return block
 
-    ring = lambda axis, block, number: Ring(place, axis, block, ring_send, ring_recv, number)
+    ring = lambda axis, block, number, direct=False: Ring(
+        place, axis, block, ring_send, ring_recv, number, direct
+    )
     tokens = [ring(2, token_block(s), s) for s in range(SEQS)]
-    wa1 = ring(1, lambda i, h: WA.at[z, i, half_rows(h)], 4)
-    wb1 = ring(0, lambda i, h: WB.at[i, y, half_rows(h)], 5)
+    wa1 = ring(1, lambda i, h: WA.at[z, i, half_rows(h)], 4, True)
+    wb1 = ring(0, lambda i, h: WB.at[i, y, half_rows(h)], 5, True)
     shifted = lambda i, k: lax.rem(i + k, 4)
     wa2 = [ring(0, lambda i, h, k=k: WA.at[i, shifted(y, k), half_rows(h)], 6 + k) for k in range(4)]
     wb2 = [ring(1, lambda i, h, k=k: WB.at[shifted(z, k), i, half_rows(h)], 10 + k) for k in range(4)]
@@ -201,17 +214,19 @@
         2,
         lambda i, h: OY.at[y, half_rows(h), pl.ds(pl.multiple_of(i * LANES, LANES), LANES)],
         14,
+        True,
     )
     oy = ring(1, lambda i, h: OY.at[i, half_rows(h)], 15)
-    oz = ring(
-        0,
-        lambda i, h: O.at[
-            c,
-            slice(None) if h is None else slice(256 * h, 256 * h + 256),
-            pl.ds(pl.multiple_of(i * 256, 256), 256),
-        ],
-        16,
-    )
+    def out_block(p):
+        def block(i, half):
+            rows = slice(256 * p, 256 * p + 256)
+            if half is not None:
+                rows = slice(256 * p + 128 * half, 256 * p + 128 * half + 128)
+            return O.at[c, rows, pl.ds(pl.multiple_of(i * 256, 256), 256)]
+
+        return block
+
+    oz = [ring(0, out_block(p), 16 + p) for p in range(2)]
 
     def pair_copy(s, k, core):
         i, half = (
@@ -260,27 +275,26 @@
     wb1.near()
     wb2[1].own()
     wb2[3].own()
-    wa2[0].near()
-    wb2[0].near()
-    ox.near()
-    token_near(0)
-    token_own(2)
     wa1.last()
     wa2[2].own()
     wb1.last()
     wb2[2].own()
+    wa2[0].near()
+    wb2[0].near()
+    ox.near()
+    ox.last()
+    token_near(0)
+    token_own(2)
     wa2[1].near()
     wa2[3].near()
     wb2[1].near()
     wb2[3].near()
-    ox.last()
     oy.own()
+    token_near(1)
+    token_own(3)
     wa2[2].near()
     wb2[2].near()
     token_last(0)
-    token_near(1)
-    token_own(3)
-    oy.near()
     wa2[0].last()
     wa2[1].last()
     wa2[3].last()
@@ -308,9 +322,24 @@
             following,
         )
 
+    def token_pair(s, first, last):
+        for k in range(first, last):
+            pair_copy(s, k, other).wait_recv()
+
+    def halo_in(s):
+        halo(s).wait_recv()
+
+    def state_in(s):
+        remote(
+            SS.at[s, 0:15], RS.at[s, 0:15], state_send.at[s], state_recv.at[s], partner
+        ).wait_recv()
+
+    def back_in(s):
+        remote(
+            SR.at[s, 0:15], RR.at[s, 0:15], back_send.at[s], back_recv.at[s], partner
+        ).wait_recv()
+
     def project(s):
-        for k in range(5):
-            pair_copy(s, k, other).wait_recv()
         product = matmul(T[s], WA[...].reshape(WIDTH, 256))
         E[s, 0, 8 : SPAN + 8, :] = product[:, 0:128]
         E[s, 1, 8 : SPAN + 8, :] = product[:, 128:256]
@@ -330,7 +359,6 @@
             CUM[s, rows, :] = matmul(ones_below, XS[s, rows, :])
 
     def convolve(s):
-        halo(s).wait_recv()
         for k in range(3):
             E[s, k, 0:8, :] = jnp.where(sp == 0, 0.0, E[s, k, 0:8, :])
         for k, taps_ref in enumerate((xt_ref, bt_ref, ct_ref)):
@@ -377,9 +405,6 @@
             Y[s, rows, :] = matmul(scores, XS[s, rows, :])
 
     def scan(s):
-        remote(
-            SS.at[s, 0:15], RS.at[s, 0:15], state_send.at[s], state_recv.at[s], partner
-        ).wait_recv()
         entering = jnp.zeros((8, LANES), F32)
         for i in range(16):
             SR[s, i] = entering
@@ -397,9 +422,6 @@
         RR[s, sp] = SR[s, sp]
 
     def finish(s):
-        remote(
-            SR.at[s, 0:15], RR.at[s, 0:15], back_send.at[s], back_recv.at[s], partner
-        ).wait_recv()
         entering = RR[s].reshape(LANES, LANES)
         for k in range(2):
             rows = slice(k * CHUNK, (k + 1) * CHUNK)
@@ -440,8 +462,6 @@
         own(s).wait()
 
     def multiply(first, last):
-        for s in range(first, last):
-            mixed_in(s)
         gathered = G[first:last].reshape((last - first) * ROWS, WIDTH)
         result = matmul(gathered, O[...].reshape(WIDTH, WIDTH))
         out_ref[first:last] = result.astype(BF16).reshape(last - first, ROWS, WIDTH)
@@ -450,46 +470,70 @@
         block = OY[...].reshape(256, 512).astype(F32).T.astype(BF16)
         O[c, :, pl.ds(pl.multiple_of(z * 256, 256), 256)] = block
 
+    token_pair(0, 0, 5)
     project(0)
     token_near(2)
+    token_last(1)
+    oy.near()
+    token_pair(1, 0, 5)
+    project(1)
+    token_near(3)
+    token_last(2)
     oy.last()
     turn()
-    oz.own()
-    token_last(1)
-    project(1)
+    oz[0].own()
+    halo_in(0)
     convolve(0)
     states(0)
-    token_near(3)
-    oz.near()
+    token_pair(2, 0, 5)
+    project(2)
+    token_last(3)
+    oz[1].own()
+    halo_in(1)
     convolve(1)
     states(1)
-    inside(0)
-    token_last(2)
-    project(2)
-    scan(0)
-    inside(1)
-    scan(1)
+    oz[0].near()
+    token_pair(3, 0, 5)
+    project(3)
+    halo_in(2)
     convolve(2)
     states(2)
-    oz.last()
-    out_pair(c).start()
-    token_last(3)
-    project(3)
-    finish(0)
-    finish(1)
+    oz[1].near()
+    state_in(0)
+    scan(0)
+    inside(0)
+    state_in(1)
+    scan(1)
+    halo_in(3)
     convolve(3)
     states(3)
+    state_in(2)
     scan(2)
+    inside(1)
     inside(2)
     inside(3)
+    back_in(0)
+    finish(0)
+    back_in(1)
+    finish(1)
+    oz[0].last()
+    oz[1].last()
+    out_pair(c).start()
+    state_in(3)
+    scan(3)
+    back_in(2)
     finish(2)
-    scan(3)
     out_pair(other).wait_recv()
+    mixed_in(0)
+    mixed_in(1)
+    mixed_in(2)
     multiply(0, 3)
+    back_in(3)
     finish(3)
+    mixed_in(3)
     multiply(3, 4)
 
-    for each in (*tokens, wa1, wb1, *wa2, *wb2, ox, oy, oz):
+    for each in (*tokens, wa1, wb1, *wa2, *wb2, ox, oy, *oz):
         each.drain()
     out_pair(c).wait_send()
     for s in range(SEQS):
@@ -552,8 +596,8 @@
             pltpu.VMEM((SEQS, 16, 8, LANES), F32),
             pltpu.VMEM((SEQS, SPAN, LANES), BF16),
             pltpu.VMEM((SEQS, ROWS, WIDTH), BF16),
-            dma((17, 4)),
-            dma((17, 4)),
+            dma((18, 4)),
+            dma((18, 4)),
             dma((SEQS + 1, 5)),
             dma((SEQS + 1, 5)),
             dma((SEQS,)),

time: 67.9 us -> 59.3 us (0.87)
  Pallas kernels: 65.8 us -> 57.3 us
    pallas_call x1, Pallas kernels: 65.8 us -> 57.3 us  [local(): pl.pallas_call(kernel, out_shape=jax.ShapeDtypeStruct(tokens.shape, BF16)...]
where the time goes in v4:
time: 59.3 us; the launch traced here: 59.1 us
  Pallas kernels  57.3 us (97%)
  local copies, waits for them, and re-layouts  1.87 us (3%)
    pallas_call x1, Pallas kernels, local(): pl.pallas_call(kernel, out_shape=jax.ShapeDtypeStruct(tokens.shape, BF16)...  57.3 us
    unnamed x1, local copies, waits for them, and re-layouts  1.87 us

profile of v4, /device:TPU:1, one launch (start us, length us, event | category | flops | bytes accessed | tf_op | source)
XLA Modules:
  0.0 59.1 jit_solution(13264918609695403145)
XLA Ops:
  0.0 57.3 %mixer.1 = bf16[4,64,1024]{2,1,0:T(8,128)(2,1)} custom-call(f32[2]{0:T(128)} %bias_ref.1, f32[2]{0:T(128)} %rate_ref.1, bf16[4,64,1024]{2,1,0:T(8,128)(2,1)} %tokens_ref.1, f32[1,1024]{1,0:T(1,128)} %bitcast.5, bf16[64,128]{1,0:T(8,128)(2,1)} %xw_ref.1, bf16[64,128]{1,0:T(8,128)(2,1)} %zw_ref.1, bf16[64,128]{1,0:T(8,128)(2,1)} %bw_ref.1, ...), custom_call_target="tpu_custom_call" | custom-call | tf_op jit(solution)/shard_map/mixer/pallas_call | solution.py:573
  57.3 1.9 %copy.16 = bf16[4,64,1024]{2,1,0:T(8,128)(2,1)} copy(bf16[4,64,1024]{2,1,0:T(8,128)(2,1)} %mixer.1) | data formatting | bytes 1048576

commit v5 on v4

--- a/solution.py
+++ b/solution.py
@@ -100,25 +100,33 @@
 
 
 def kernel(
+    bias_in,
+    rate_in,
+    tokens_in,
+    gain_in,
+    xw_in,
+    zw_in,
+    bw_in,
+    cw_in,
+    dw_in,
+    xt_in,
+    bt_in,
+    ct_in,
+    og_in,
+    ow_in,
+    out_hbm,
     bias_ref,
     rate_ref,
     tokens_ref,
     gain_ref,
-    xw_ref,
-    zw_ref,
-    bw_ref,
-    cw_ref,
     dw_ref,
-    xt_ref,
-    bt_ref,
-    ct_ref,
+    taps_ref,
     og_ref,
-    ow_ref,
     out_ref,
     T,
     WA,
     WB,
-    OY,
+    OYZ,
     O,
     E,
     Z,
@@ -148,6 +156,8 @@
     mix_send,
     mix_recv,
     local_sem,
+    load_sem,
+    out_sem,
 ):
     z, y = lax.axis_index("sp_0"), lax.axis_index("sp_1")
     x, c = lax.axis_index("tp_0"), lax.axis_index("tp_1")
@@ -169,28 +179,45 @@
             pl.semaphore_signal(barrier, inc=1, device_id=near, device_id_type=MESH)
     pl.semaphore_signal(barrier, inc=1, device_id=partner, device_id_type=MESH)
 
+    loads = (
+        (xw_in, WA.at[z, y, :, 0:128]),
+        (bw_in, WA.at[z, y, :, 128:256]),
+        (cw_in, WB.at[z, y, :, 0:128]),
+        (zw_in, WB.at[z, y, :, 128:256]),
+        (dw_in, dw_ref),
+        (ow_in, OYZ.at[z, y]),
+        (gain_in, gain_ref),
+        *((tokens_in.at[s], tokens_ref.at[s]) for s in range(SEQS)),
+        (xt_in, taps_ref.at[0]),
+        (bt_in, taps_ref.at[1]),
+        (ct_in, taps_ref.at[2]),
+        (og_in, og_ref),
+        (bias_in, bias_ref),
+        (rate_in, rate_ref),
+    )
+    loads = [pltpu.make_async_copy(*pair, load_sem.at[k]) for k, pair in enumerate(loads)]
+    for load in loads:
+        load.start()
+
     lane = lax.broadcasted_iota(jnp.int32, (1, LANES), 1)
     low = lane < 64
 
-    WA[z, y, :, 0:128] = xw_ref[...]
-    WA[z, y, :, 128:256] = bw_ref[...]
-    WB[z, y, :, 0:128] = cw_ref[...]
-    WB[z, y, :, 128:256] = zw_ref[...]
     head_at = lax.broadcasted_iota(jnp.int32, (2, LANES), 0)
     lane_at = lax.broadcasted_iota(jnp.int32, (2, LANES), 1)
     spread = (lane_at // 64 == head_at).astype(BF16)
+    for load in loads[0:7]:
+        load.wait()
     WB[z, y, :, 256:384] = matmul(dw_ref[...], spread, ((0,), (0,))).astype(BF16)
 
     def normed(s):
+        loads[7 + s].wait()
         source = tokens_ref[s].astype(F32)
         scale = lax.rsqrt(jnp.mean(source * source, axis=-1, keepdims=True) + epsilon)
         T[s, pl.ds(pl.multiple_of(tp * ROWS, ROWS), ROWS), :] = (
             source * scale * gain_ref[...]
         ).astype(BF16)
 
-    normed(0)
     own_columns = pl.multiple_of((c * 4 + x) * LANES, LANES)
-    OY[y, :, pl.ds(pl.multiple_of(x * LANES, LANES), LANES)] = ow_ref[...]
     pl.semaphore_wait(barrier, 10)
 
     def token_block(s):
@@ -210,23 +237,15 @@
     shifted = lambda i, k: lax.rem(i + k, 4)
     wa2 = [ring(0, lambda i, h, k=k: WA.at[i, shifted(y, k), half_rows(h)], 6 + k) for k in range(4)]
     wb2 = [ring(1, lambda i, h, k=k: WB.at[shifted(z, k), i, half_rows(h)], 10 + k) for k in range(4)]
-    ox = ring(
-        2,
-        lambda i, h: OY.at[y, half_rows(h), pl.ds(pl.multiple_of(i * LANES, LANES), LANES)],
-        14,
-        True,
-    )
-    oy = ring(1, lambda i, h: OY.at[i, half_rows(h)], 15)
-    def out_block(p):
-        def block(i, half):
-            rows = slice(256 * p, 256 * p + 256)
-            if half is not None:
-                rows = slice(256 * p + 128 * half, 256 * p + 128 * half + 128)
-            return O.at[c, rows, pl.ds(pl.multiple_of(i * 256, 256), 256)]
-
-        return block
-
-    oz = [ring(0, out_block(p), 16 + p) for p in range(2)]
+    oy = ring(1, lambda i, h: OYZ.at[z, i], 14, True)
+    oz = ring(0, lambda i, h: OYZ.at[i, half_blocks(h)], 15)
+
+    def out_rows(core, i, half):
+        rows = LANES if half is None else 64
+        start = i * LANES + (0 if half is None else 64 * half)
+        return O.at[core, pl.ds(pl.multiple_of(start, 64), rows), :]
+
+    ox = ring(2, lambda i, h: out_rows(c, i, h), 16)
 
     def pair_copy(s, k, core):
         i, half = (
@@ -241,9 +260,30 @@
         ref = T.at[s, pl.ds(pl.multiple_of(start, 32), rows), :]
         return remote(ref, ref, pair_send.at[s, k], pair_recv.at[s, k], partner)
 
-    def out_pair(core):
-        ref = O.at[core]
-        return remote(ref, ref, pair_send.at[SEQS, 0], pair_recv.at[SEQS, 0], partner)
+    def out_pair(k, core):
+        i, half = ((x, None), (ox.left, None), (ox.right, None), (ox.far, 0), (ox.far, 1))[k]
+        ref = out_rows(core, i, half)
+        return remote(ref, ref, pair_send.at[SEQS, k], pair_recv.at[SEQS, k], partner)
+
+    def out_own():
+        block = OYZ[...].reshape(WIDTH, LANES).astype(F32).T.astype(BF16)
+        O[c, pl.ds(pl.multiple_of(x * LANES, LANES), LANES), :] = block
+        ox.own()
+        out_pair(0, c).start()
+
+    def out_near():
+        ox.near()
+        out_pair(1, c).start()
+        out_pair(2, c).start()
+
+    def out_last():
+        ox.last()
+        out_pair(3, c).start()
+        out_pair(4, c).start()
+
+    def out_pairs():
+        for k in range(5):
+            out_pair(k, other).wait_recv()
 
     def token_own(s):
         tokens[s].own()
@@ -263,7 +303,7 @@
     wb1.own()
     wa2[0].own()
     wb2[0].own()
-    ox.own()
+    normed(0)
     token_own(0)
     normed(1)
     token_own(1)
@@ -281,8 +321,6 @@
     wb2[2].own()
     wa2[0].near()
     wb2[0].near()
-    ox.near()
-    ox.last()
     token_near(0)
     token_own(2)
     wa2[1].near()
@@ -298,12 +336,19 @@
     wa2[0].last()
     wa2[1].last()
     wa2[3].last()
-    wa2[2].last()
     wb2[0].last()
     wb2[1].last()
     wb2[3].last()
+    oy.near()
+    oy.last()
+    oz.own()
+    token_near(2)
+    token_last(1)
+    wa2[2].last()
     wb2[2].last()
 
+    for load in loads[11:]:
+        load.wait()
     bias = jnp.where(low, bias_ref[0], bias_ref[1])
     rate = jnp.where(low, rate_ref[0], rate_ref[1])
     row_at = lax.broadcasted_iota(jnp.int32, (CHUNK, CHUNK), 0)
@@ -361,8 +406,8 @@
     def convolve(s):
         for k in range(3):
             E[s, k, 0:8, :] = jnp.where(sp == 0, 0.0, E[s, k, 0:8, :])
-        for k, taps_ref in enumerate((xt_ref, bt_ref, ct_ref)):
-            taps = [taps_ref[offset : offset + 1, :] for offset in range(CONV)]
+        for k in range(3):
+            taps = [taps_ref[k, offset : offset + 1, :] for offset in range(CONV)]
             for rows in tiles:
                 start = rows.start + 5
                 running = taps[0] * E[s, k, start : start + ROWS, :]
@@ -461,81 +506,79 @@
         ).wait_recv()
         own(s).wait()
 
+    def put_out(first, last):
+        return pltpu.make_async_copy(
+            out_ref.at[first:last], out_hbm.at[first:last], out_sem.at[first]
+        )
+
     def multiply(first, last):
         gathered = G[first:last].reshape((last - first) * ROWS, WIDTH)
         result = matmul(gathered, O[...].reshape(WIDTH, WIDTH))
         out_ref[first:last] = result.astype(BF16).reshape(last - first, ROWS, WIDTH)
-
-    def turn():
-        block = OY[...].reshape(256, 512).astype(F32).T.astype(BF16)
-        O[c, :, pl.ds(pl.multiple_of(z * 256, 256), 256)] = block
+        put_out(first, last).start()
 
     token_pair(0, 0, 5)
     project(0)
-    token_near(2)
-    token_last(1)
-    oy.near()
+    token_near(3)
     token_pair(1, 0, 5)
     project(1)
-    token_near(3)
+    oz.near()
     token_last(2)
-    oy.last()
-    turn()
-    oz[0].own()
     halo_in(0)
     convolve(0)
     states(0)
     token_pair(2, 0, 5)
     project(2)
-    token_last(3)
-    oz[1].own()
+    oz.last()
+    out_own()
     halo_in(1)
     convolve(1)
     states(1)
-    oz[0].near()
+    token_last(3)
+    state_in(0)
+    scan(0)
     token_pair(3, 0, 5)
     project(3)
     halo_in(2)
     convolve(2)
     states(2)
-    oz[1].near()
-    state_in(0)
-    scan(0)
     inside(0)
     state_in(1)
     scan(1)
+    out_near()
     halo_in(3)
     convolve(3)
     states(3)
+    back_in(0)
+    finish(0)
+    inside(1)
     state_in(2)
     scan(2)
-    inside(1)
+    back_in(1)
+    finish(1)
     inside(2)
     inside(3)
-    back_in(0)
-    finish(0)
-    back_in(1)
-    finish(1)
-    oz[0].last()
-    oz[1].last()
-    out_pair(c).start()
+    out_last()
     state_in(3)
     scan(3)
     back_in(2)
     finish(2)
-    out_pair(other).wait_recv()
+    back_in(3)
+    finish(3)
+    out_pairs()
     mixed_in(0)
     mixed_in(1)
     mixed_in(2)
     multiply(0, 3)
-    back_in(3)
-    finish(3)
     mixed_in(3)
     multiply(3, 4)
 
-    for each in (*tokens, wa1, wb1, *wa2, *wb2, ox, oy, *oz):
+    for each in (*tokens, wa1, wb1, *wa2, *wb2, oy, oz, ox):
         each.drain()
-    out_pair(c).wait_send()
+    for k in range(5):
+        out_pair(k, c).wait_send()
+    put_out(0, 3).wait()
+    put_out(3, 4).wait()
     for s in range(SEQS):
         for k in range(5):
             pair_copy(s, k, c).wait_send()
@@ -567,19 +610,26 @@
     out_gain,
     out_weight,
 ):
-    smem = pl.BlockSpec(memory_space=pltpu.SMEM)
-    vmem = pl.BlockSpec(memory_space=pltpu.VMEM)
+    hbm = pl.BlockSpec(memory_space=pltpu.HBM)
     dma = pltpu.SemaphoreType.DMA
     return pl.pallas_call(
         kernel,
         out_shape=jax.ShapeDtypeStruct(tokens.shape, BF16),
-        in_specs=[smem, smem] + [vmem] * 12,
-        out_specs=vmem,
+        in_specs=[hbm] * 14,
+        out_specs=hbm,
         scratch_shapes=[
+            pltpu.SMEM((2,), F32),
+            pltpu.SMEM((2,), F32),
+            pltpu.VMEM((SEQS, ROWS, WIDTH), BF16),
+            pltpu.VMEM((1, WIDTH), F32),
+            pltpu.VMEM((2, ROWS), BF16),
+            pltpu.VMEM((3, CONV, LANES), F32),
+            pltpu.VMEM((1, LANES), F32),
+            pltpu.VMEM((SEQS, ROWS, WIDTH), BF16),
             pltpu.VMEM((SEQS, SPAN, WIDTH), BF16),
             pltpu.VMEM((4, 4, ROWS, 256), BF16),
             pltpu.VMEM((4, 4, ROWS, 384), BF16),
-            pltpu.VMEM((4, ROWS, 512), BF16),
+            pltpu.VMEM((4, 4, ROWS, LANES), BF16),
             pltpu.VMEM((2, 512, WIDTH), BF16),
             pltpu.VMEM((SEQS, 3, SPAN + 8, LANES), F32),
             pltpu.VMEM((SEQS, SPAN, LANES), F32),
@@ -596,8 +646,8 @@
             pltpu.VMEM((SEQS, 16, 8, LANES), F32),
             pltpu.VMEM((SEQS, SPAN, LANES), BF16),
             pltpu.VMEM((SEQS, ROWS, WIDTH), BF16),
-            dma((18, 4)),
-            dma((18, 4)),
+            dma((17, 4)),
+            dma((17, 4)),
             dma((SEQS + 1, 5)),
             dma((SEQS + 1, 5)),
             dma((SEQS,)),
@@ -608,6 +658,8 @@
             dma((SEQS,)),
             dma((SEQS,)),
             dma((SEQS,)),
+            dma((SEQS,)),
+            dma((17,)),
             dma((SEQS,)),
         ],
         compiler_params=pltpu.CompilerParams(

time: 59.3 us -> 58.3 us (0.983)
  Pallas kernels: 57.3 us -> 56.3 us
    pallas_call x1, Pallas kernels: 57.3 us -> 56.3 us  [local(): pl.pallas_call(kernel, out_shape=jax.ShapeDtypeStruct(tokens.shape, BF16)...]
where the time goes in v5:
time: 58.3 us; the launch traced here: 58.2 us
  Pallas kernels  56.3 us (97%)
  local copies, waits for them, and re-layouts  1.87 us (3%)
    pallas_call x1, Pallas kernels, local(): pl.pallas_call(kernel, out_shape=jax.ShapeDtypeStruct(tokens.shape, BF16)...  56.3 us
    unnamed x1, local copies, waits for them, and re-layouts  1.87 us

profile of v5, /device:TPU:1, one launch (start us, length us, event | category | flops | bytes accessed | tf_op | source)
XLA Modules:
  0.0 58.2 jit_solution(13726170638383675029)
XLA Ops:
  0.0 56.3 %mixer.1 = bf16[4,64,1024]{2,1,0:T(8,128)(2,1)} custom-call(f32[2]{0:T(128)} %bias_in.1, f32[2]{0:T(128)} %rate_in.1, bf16[4,64,1024]{2,1,0:T(8,128)(2,1)} %tokens_in.1, f32[1,1024]{1,0:T(1,128)} %bitcast.5, bf16[64,128]{1,0:T(8,128)(2,1)} %xw_in.1, bf16[64,128]{1,0:T(8,128)(2,1)} %zw_in.1, bf16[64,128]{1,0:T(8,128)(2,1)} %bw_in.1, bf16[64,128]{1,0:T(8,128)(2,1)} %cw_in.1, ...), custom_call_target="tpu_custom_call" | custom-call | tf_op jit(solution)/shard_map/mixer/pallas_call | solution.py:615
  56.3 1.9 %copy.16 = bf16[4,64,1024]{2,1,0:T(8,128)(2,1)} copy(bf16[4,64,1024]{2,1,0:T(8,128)(2,1)} %mixer.1) | data formatting | bytes 1048576

commit v6 on v5

--- a/solution.py
+++ b/solution.py
@@ -114,7 +114,7 @@
     ct_in,
     og_in,
     ow_in,
-    out_hbm,
+    out_ref,
     bias_ref,
     rate_ref,
     tokens_ref,
@@ -122,7 +122,6 @@
     dw_ref,
     taps_ref,
     og_ref,
-    out_ref,
     T,
     WA,
     WB,
@@ -141,6 +140,7 @@
     RS,
     SR,
     RR,
+    ROW,
     GT,
     G,
     ring_send,
@@ -157,7 +157,6 @@
     mix_recv,
     local_sem,
     load_sem,
-    out_sem,
 ):
     z, y = lax.axis_index("sp_0"), lax.axis_index("sp_1")
     x, c = lax.axis_index("tp_0"), lax.axis_index("tp_1")
@@ -238,7 +237,7 @@
     wa2 = [ring(0, lambda i, h, k=k: WA.at[i, shifted(y, k), half_rows(h)], 6 + k) for k in range(4)]
     wb2 = [ring(1, lambda i, h, k=k: WB.at[shifted(z, k), i, half_rows(h)], 10 + k) for k in range(4)]
     oy = ring(1, lambda i, h: OYZ.at[z, i], 14, True)
-    oz = ring(0, lambda i, h: OYZ.at[i, half_blocks(h)], 15)
+    oz = ring(0, lambda i, h: OYZ.at[i], 15, True)
 
     def out_rows(core, i, half):
         rows = LANES if half is None else 64
@@ -303,6 +302,7 @@
     wb1.own()
     wa2[0].own()
     wb2[0].own()
+    oy.own()
     normed(0)
     token_own(0)
     normed(1)
@@ -323,13 +323,15 @@
     wb2[0].near()
     token_near(0)
     token_own(2)
+    token_own(3)
     wa2[1].near()
     wa2[3].near()
     wb2[1].near()
     wb2[3].near()
-    oy.own()
     token_near(1)
-    token_own(3)
+    oy.near()
+    oy.last()
+    oz.own()
     wa2[2].near()
     wb2[2].near()
     token_last(0)
@@ -339,11 +341,7 @@
     wb2[0].last()
     wb2[1].last()
     wb2[3].last()
-    oy.near()
-    oy.last()
-    oz.own()
     token_near(2)
-    token_last(1)
     wa2[2].last()
     wb2[2].last()
 
@@ -358,6 +356,16 @@
     tiles = [slice(k * ROWS, (k + 1) * ROWS) for k in range(SPAN // ROWS)]
     following = sp_device(lax.rem(sp + 1, 16))
 
+    def packed(state, log):
+        log = jnp.broadcast_to(log, (16, LANES))
+        return jnp.concatenate([state, log], axis=0).astype(BF16)
+
+    def share(source, slots, axis, send, recv):
+        for k in (1, 3, 2):
+            there = tuple(lax.rem(p + k, 4) if j == axis else p for j, p in enumerate(place))
+            remote(source, slots.at[place[axis]], send, recv, there).start()
+        slots[place[axis]] = source[...]
+
     def halo(s):
         return remote(
             E.at[s, :, SPAN : SPAN + 8, :],
@@ -376,12 +384,12 @@
 
     def state_in(s):
         remote(
-            SS.at[s, 0:15], RS.at[s, 0:15], state_send.at[s], state_recv.at[s], partner
+            RS.at[s, 0:3], RS.at[s, 0:3], state_send.at[s], state_recv.at[s], partner
         ).wait_recv()
 
     def back_in(s):
         remote(
-            SR.at[s, 0:15], RR.at[s, 0:15], back_send.at[s], back_recv.at[s], partner
+            RR.at[s, 0:3], RR.at[s, 0:3], back_send.at[s], back_recv.at[s], partner
         ).wait_recv()
 
     def project(s):
@@ -393,8 +401,13 @@
         Z[s] = product[:, 128:256]
         DT[s] = product[:, 256:384]
         halo(s).start()
+
+    def gate(s):
         for rows in tiles:
             Z[s, rows, :] = silu(Z[s, rows, :])
+
+    def steps(s):
+        for rows in tiles:
             step = DT[s, rows, :] + bias
             step = jnp.maximum(step, 0.0) + jnp.log1p(jnp.exp(-jnp.abs(step)))
             DT[s, rows, :] = step
@@ -403,12 +416,19 @@
             rows = slice(k * CHUNK, (k + 1) * CHUNK)
             CUM[s, rows, :] = matmul(ones_below, XS[s, rows, :])
 
-    def convolve(s):
+    def conv_tail(s):
+        convolve(s, tiles[1:])
+        gains(s, 1)
+
+    def conv_head(s):
         for k in range(3):
             E[s, k, 0:8, :] = jnp.where(sp == 0, 0.0, E[s, k, 0:8, :])
+        convolve(s, tiles[:1])
+
+    def convolve(s, some):
         for k in range(3):
             taps = [taps_ref[k, offset : offset + 1, :] for offset in range(CONV)]
-            for rows in tiles:
+            for rows in some:
                 start = rows.start + 5
                 running = taps[0] * E[s, k, start : start + ROWS, :]
                 for offset in range(1, CONV):
@@ -423,24 +443,16 @@
                 else:
                     CS[s, rows, :] = running.astype(BF16)
 
+    def gains(s, k):
+        rows = slice(k * CHUNK, (k + 1) * CHUNK)
+        U[s, k] = matmul(BS[s, rows, :], XS[s, rows, :], ((0,), (0,)))
+
     def states(s):
-        for k in range(2):
-            rows = slice(k * CHUNK, (k + 1) * CHUNK)
-            U[s, k] = matmul(BS[s, rows, :], XS[s, rows, :], ((0,), (0,)))
+        gains(s, 0)
         first, second = CUM[s, CHUNK - 1 : CHUNK, :], CUM[s, SPAN - 1 : SPAN, :]
         final = jnp.exp(second) * (jnp.exp(first) * U[s, 0] + U[s, 1])
-        total = jnp.broadcast_to((first + second).reshape(1, 1, LANES), (16, 8, LANES))
-        SS[s] = jnp.concatenate([final.reshape(16, 8, LANES), total], axis=1).astype(BF16)
-
-        def send(k, _):
-            i = lax.rem(sp + k, 16)
-            remote(
-                SS.at[s, i], RS.at[s, sp], state_send.at[s], state_recv.at[s], sp_device(i)
-            ).start()
-            return 0
-
-        lax.fori_loop(1, 16, send, 0)
-        RS[s, sp] = SS[s, sp]
+        SS[s] = packed(final, first + second)
+        share(SS.at[s], RS.at[s], 1, state_send.at[s], state_recv.at[s])
 
     def inside(s):
         for k in range(2):
@@ -450,24 +462,29 @@
             Y[s, rows, :] = matmul(scores, XS[s, rows, :])
 
     def scan(s):
-        entering = jnp.zeros((8, LANES), F32)
-        for i in range(16):
-            SR[s, i] = entering
+        before, before_log = jnp.zeros((LANES, LANES), F32), jnp.zeros((1, LANES), F32)
+        total, total_log = before, before_log
+        for i in range(4):
             piece = RS[s, i].astype(F32)
-            entering = jnp.exp(piece[8:16]) * entering + piece[0:8]
-
-        def send(k, _):
-            i = lax.rem(sp + k, 16)
-            remote(
-                SR.at[s, i], RR.at[s, sp], back_send.at[s], back_recv.at[s], sp_device(i)
-            ).start()
-            return 0
-
-        lax.fori_loop(1, 16, send, 0)
-        RR[s, sp] = SR[s, sp]
+            log = piece[LANES : LANES + 1]
+            total = jnp.exp(log) * total + piece[0:LANES]
+            total_log = total_log + log
+            if i < 3:
+                before = jnp.where(i + 1 == y, total, before)
+                before_log = jnp.where(i + 1 == y, total_log, before_log)
+        ROW[s, 0:LANES] = before
+        ROW[s, LANES : LANES + 1] = jnp.exp(before_log)
+        SR[s] = packed(total, total_log)
+        share(SR.at[s], RR.at[s], 0, back_send.at[s], back_recv.at[s])
 
     def finish(s):
-        entering = RR[s].reshape(LANES, LANES)
+        total = jnp.zeros((LANES, LANES), F32)
+        entering = total
+        for i in range(3):
+            piece = RR[s, i].astype(F32)
+            total = jnp.exp(piece[LANES : LANES + 1]) * total + piece[0:LANES]
+            entering = jnp.where(i + 1 == z, total, entering)
+        entering = ROW[s, LANES : LANES + 1] * entering + ROW[s, 0:LANES]
         for k in range(2):
             rows = slice(k * CHUNK, (k + 1) * CHUNK)
             Y[s, rows, :] += matmul(CS[s, rows, :], entering.astype(BF16))
@@ -506,61 +523,68 @@
         ).wait_recv()
         own(s).wait()
 
-    def put_out(first, last):
-        return pltpu.make_async_copy(
-            out_ref.at[first:last], out_hbm.at[first:last], out_sem.at[first]
-        )
-
     def multiply(first, last):
         gathered = G[first:last].reshape((last - first) * ROWS, WIDTH)
         result = matmul(gathered, O[...].reshape(WIDTH, WIDTH))
         out_ref[first:last] = result.astype(BF16).reshape(last - first, ROWS, WIDTH)
-        put_out(first, last).start()
 
     token_pair(0, 0, 5)
     project(0)
+    steps(0)
+    conv_tail(0)
     token_near(3)
+    oz.near()
+    oz.last()
+    out_own()
+    token_last(1)
+    halo_in(0)
+    conv_head(0)
+    states(0)
+    token_last(2)
+    inside(0)
+    gate(0)
     token_pair(1, 0, 5)
     project(1)
-    oz.near()
-    token_last(2)
-    halo_in(0)
-    convolve(0)
-    states(0)
+    token_last(3)
     token_pair(2, 0, 5)
     project(2)
-    oz.last()
-    out_own()
+    steps(1)
+    conv_tail(1)
     halo_in(1)
-    convolve(1)
+    conv_head(1)
     states(1)
-    token_last(3)
+    token_pair(3, 0, 5)
+    project(3)
     state_in(0)
     scan(0)
-    token_pair(3, 0, 5)
-    project(3)
+    steps(2)
+    conv_tail(2)
     halo_in(2)
-    convolve(2)
+    conv_head(2)
     states(2)
-    inside(0)
+    steps(3)
+    conv_tail(3)
+    halo_in(3)
+    conv_head(3)
+    states(3)
+    out_near()
     state_in(1)
     scan(1)
-    out_near()
-    halo_in(3)
-    convolve(3)
-    states(3)
     back_in(0)
     finish(0)
+    gate(1)
     inside(1)
     state_in(2)
     scan(2)
+    gate(2)
+    inside(2)
+    gate(3)
+    inside(3)
+    state_in(3)
+    scan(3)
     back_in(1)
     finish(1)
-    inside(2)
-    inside(3)
     out_last()
-    state_in(3)
-    scan(3)
     back_in(2)
     finish(2)
     back_in(3)
@@ -577,17 +601,15 @@
         each.drain()
     for k in range(5):
         out_pair(k, c).wait_send()
-    put_out(0, 3).wait()
-    put_out(3, 4).wait()
     for s in range(SEQS):
         for k in range(5):
             pair_copy(s, k, c).wait_send()
         halo(s).wait_send()
         remote(
-            SS.at[s, 0:15], RS.at[s, 0:15], state_send.at[s], state_recv.at[s], partner
+            RS.at[s, 0:3], RS.at[s, 0:3], state_send.at[s], state_recv.at[s], partner
         ).wait_send()
         remote(
-            SR.at[s, 0:15], RR.at[s, 0:15], back_send.at[s], back_recv.at[s], partner
+            RR.at[s, 0:3], RR.at[s, 0:3], back_send.at[s], back_recv.at[s], partner
         ).wait_send()
         remote(
             G.at[s, :, 0:896], G.at[s, :, 0:896], mix_send.at[s], mix_recv.at[s], partner
@@ -614,9 +636,9 @@
     dma = pltpu.SemaphoreType.DMA
     return pl.pallas_call(
         kernel,
-        out_shape=jax.ShapeDtypeStruct(tokens.shape, BF16),
+        out_shape=pltpu.VMEM(tokens.shape, BF16),
         in_specs=[hbm] * 14,
-        out_specs=hbm,
+        out_specs=pl.BlockSpec(memory_space=pltpu.VMEM),
         scratch_shapes=[
             pltpu.SMEM((2,), F32),
             pltpu.SMEM((2,), F32),
@@ -625,7 +647,6 @@
             pltpu.VMEM((2, ROWS), BF16),
             pltpu.VMEM((3, CONV, LANES), F32),
             pltpu.VMEM((1, LANES), F32),
-            pltpu.VMEM((SEQS, ROWS, WIDTH), BF16),
             pltpu.VMEM((SEQS, SPAN, WIDTH), BF16),
             pltpu.VMEM((4, 4, ROWS, 256), BF16),
             pltpu.VMEM((4, 4, ROWS, 384), BF16),
@@ -640,10 +661,11 @@
             pltpu.VMEM((SEQS, SPAN, LANES), BF16),
             pltpu.VMEM((SEQS, SPAN, LANES), F32),
             pltpu.VMEM((SEQS, 2, LANES, LANES), F32),
-            pltpu.VMEM((SEQS, 16, 16, LANES), BF16),
-            pltpu.VMEM((SEQS, 16, 16, LANES), BF16),
-            pltpu.VMEM((SEQS, 16, 8, LANES), F32),
-            pltpu.VMEM((SEQS, 16, 8, LANES), F32),
+            pltpu.VMEM((SEQS, LANES + 16, LANES), BF16),
+            pltpu.VMEM((SEQS, 4, LANES + 16, LANES), BF16),
+            pltpu.VMEM((SEQS, LANES + 16, LANES), BF16),
+            pltpu.VMEM((SEQS, 4, LANES + 16, LANES), BF16),
+            pltpu.VMEM((SEQS, LANES + 8, LANES), F32),
             pltpu.VMEM((SEQS, SPAN, LANES), BF16),
             pltpu.VMEM((SEQS, ROWS, WIDTH), BF16),
             dma((17, 4)),
@@ -660,10 +682,9 @@
             dma((SEQS,)),
             dma((SEQS,)),
             dma((17,)),
-            dma((SEQS,)),
         ],
         compiler_params=pltpu.CompilerParams(
-            collective_id=0, has_side_effects=True, vmem_limit_bytes=56 * 1024 * 1024
+            collective_id=0, has_side_effects=True, vmem_limit_bytes=60 * 1024 * 1024
         ),
         name="mixer",
     )(

time: 58.3 us -> 51.8 us (0.89)
  Pallas kernels: 56.3 us -> 50.8 us
  local copies, waits for them, and re-layouts: 1.87 us -> 0.8 us
    pallas_call x1, Pallas kernels: 56.3 us -> 50.8 us  [local(): pl.pallas_call(kernel, out_shape=pltpu.VMEM(tokens.shape, BF16), in_specs...]
    unnamed x1, local copies, waits for them, and re-layouts: 1.87 us -> 0.8 us
where the time goes in v6:
time: 51.8 us; the launch traced here: 51.6 us
  Pallas kernels  50.8 us (98%)
  local copies, waits for them, and re-layouts  0.8 us (2%)
    pallas_call x1, Pallas kernels, local(): pl.pallas_call(kernel, out_shape=pltpu.VMEM(tokens.shape, BF16), in_specs...  50.8 us

profile of v6, /device:TPU:1, one launch (start us, length us, event | category | flops | bytes accessed | tf_op | source)
XLA Modules:
  0.0 51.6 jit_solution(10849166234874751234)
XLA Ops:
  0.0 50.8 %mixer.1 = bf16[4,64,1024]{2,1,0:T(8,128)(2,1)S(1)} custom-call(f32[2]{0:T(128)} %bias_in.1, f32[2]{0:T(128)} %rate_in.1, bf16[4,64,1024]{2,1,0:T(8,128)(2,1)} %tokens_in.1, f32[1,1024]{1,0:T(1,128)} %bitcast.5, bf16[64,128]{1,0:T(8,128)(2,1)} %xw_in.1, bf16[64,128]{1,0:T(8,128)(2,1)} %zw_in.1, bf16[64,128]{1,0:T(8,128)(2,1)} %bw_in.1, ...), custom_call_target="tpu_custom_call" | custom-call | tf_op jit(solution)/shard_map/mixer/pallas_call | solution.py:637
  50.9 0.8 %copy.16 = bf16[4,64,1024]{2,1,0:T(8,128)(2,1)} copy(bf16[4,64,1024]{2,1,0:T(8,128)(2,1)S(1)} %mixer.1) | data formatting | bytes 1048576

commit v7 on v6

--- a/solution.py
+++ b/solution.py
@@ -157,6 +157,7 @@
     mix_recv,
     local_sem,
     load_sem,
+    ready_sem,
 ):
     z, y = lax.axis_index("sp_0"), lax.axis_index("sp_1")
     x, c = lax.axis_index("tp_0"), lax.axis_index("tp_1")
@@ -172,11 +173,16 @@
         return (z, y, i // 2, lax.rem(i, 2))
 
     barrier = pltpu.get_barrier_semaphore()
+
+    def greet(semaphore, there):
+        pl.semaphore_signal(semaphore, inc=1, device_id=there, device_id_type=MESH)
+
+    for step in (1, 3):
+        greet(barrier, (z, y, lax.rem(x + step, 4), c))
+    greet(barrier, partner)
     for step in (1, 2, 3):
-        for axis in range(3):
-            near = tuple(lax.rem(p + step, 4) if k == axis else p for k, p in enumerate(place))
-            pl.semaphore_signal(barrier, inc=1, device_id=near, device_id_type=MESH)
-    pl.semaphore_signal(barrier, inc=1, device_id=partner, device_id_type=MESH)
+        pl.when(y + step < 4)(lambda step=step: greet(barrier, (z, y + step, x, c)))
+        pl.when(z + step < 4)(lambda step=step: greet(barrier, (z + step, y, x, c)))
 
     loads = (
         (xw_in, WA.at[z, y, :, 0:128]),
@@ -217,7 +223,10 @@
         ).astype(BF16)
 
     own_columns = pl.multiple_of((c * 4 + x) * LANES, LANES)
-    pl.semaphore_wait(barrier, 10)
+    pl.semaphore_wait(barrier, 3 + y + z)
+    for step in (1, 2, 3):
+        pl.when(y >= step)(lambda step=step: greet(ready_sem, (z, y - step, x, c)))
+        pl.when(z >= step)(lambda step=step: greet(ready_sem, (z - step, y, x, c)))
 
     def token_block(s):
         def block(i, half):
@@ -298,13 +307,14 @@
         pair_copy(s, 3, c).start()
         pair_copy(s, 4, c).start()
 
+    normed(0)
+    token_own(0)
+    pl.when(y + z < 6)(lambda: pl.semaphore_wait(ready_sem, 6 - y - z))
     wa1.own()
     wb1.own()
     wa2[0].own()
     wb2[0].own()
     oy.own()
-    normed(0)
-    token_own(0)
     normed(1)
     token_own(1)
     normed(2)
@@ -360,11 +370,27 @@
         log = jnp.broadcast_to(log, (16, LANES))
         return jnp.concatenate([state, log], axis=0).astype(BF16)
 
-    def share(source, slots, axis, send, recv):
+    def share_row(s):
         for k in (1, 3, 2):
-            there = tuple(lax.rem(p + k, 4) if j == axis else p for j, p in enumerate(place))
-            remote(source, slots.at[place[axis]], send, recv, there).start()
-        slots[place[axis]] = source[...]
+            there = (z, lax.rem(y + k, 4), x, c)
+            copy = remote(SS.at[s], RS.at[s, y], state_send.at[s, k], state_recv.at[s, y], there)
+            pl.when((y + k < 4) | (z < 3))(copy.start)
+        RS[s, y] = SS[s]
+
+    def share_up(s):
+        for k in (1, 2, 3):
+            there = (lax.rem(z + k, 4), y, x, c)
+            copy = remote(SR.at[s], RR.at[s, z], back_send.at[s, k], back_recv.at[s, z], there)
+            pl.when(z + k < 4)(copy.start)
+
+    def states_out(s):
+        for k in (1, 3, 2):
+            copy = remote(
+                SS.at[s], RS.at[s, y], state_send.at[s, k], state_recv.at[s, y], partner
+            )
+            pl.when((y + k < 4) | (z < 3))(copy.wait_send)
+            copy = remote(SR.at[s], RR.at[s, z], back_send.at[s, k], back_recv.at[s, z], partner)
+            pl.when(z + k < 4)(copy.wait_send)
 
     def halo(s):
         return remote(
@@ -380,17 +406,20 @@
             pair_copy(s, k, other).wait_recv()
 
     def halo_in(s):
-        halo(s).wait_recv()
+        pl.when(sp > 0)(halo(s).wait_recv)
 
     def state_in(s):
-        remote(
-            RS.at[s, 0:3], RS.at[s, 0:3], state_send.at[s], state_recv.at[s], partner
-        ).wait_recv()
+        for k in (1, 3, 2):
+            i = lax.rem(y + k, 4)
+            copy = remote(
+                SS.at[s], RS.at[s, i], state_send.at[s, k], state_recv.at[s, i], partner
+            )
+            pl.when((i < y) | (z < 3))(copy.wait_recv)
 
     def back_in(s):
-        remote(
-            RR.at[s, 0:3], RR.at[s, 0:3], back_send.at[s], back_recv.at[s], partner
-        ).wait_recv()
+        for i in range(3):
+            copy = remote(SR.at[s], RR.at[s, i], back_send.at[s, 0], back_recv.at[s, i], partner)
+            pl.when(i < z)(copy.wait_recv)
 
     def project(s):
         product = matmul(T[s], WA[...].reshape(WIDTH, 256))
@@ -400,7 +429,7 @@
         E[s, 2, 8 : SPAN + 8, :] = product[:, 0:128]
         Z[s] = product[:, 128:256]
         DT[s] = product[:, 256:384]
-        halo(s).start()
+        pl.when(sp < 15)(halo(s).start)
 
     def gate(s):
         for rows in tiles:
@@ -452,7 +481,7 @@
         first, second = CUM[s, CHUNK - 1 : CHUNK, :], CUM[s, SPAN - 1 : SPAN, :]
         final = jnp.exp(second) * (jnp.exp(first) * U[s, 0] + U[s, 1])
         SS[s] = packed(final, first + second)
-        share(SS.at[s], RS.at[s], 1, state_send.at[s], state_recv.at[s])
+        share_row(s)
 
     def inside(s):
         for k in range(2):
@@ -475,7 +504,7 @@
         ROW[s, 0:LANES] = before
         ROW[s, LANES : LANES + 1] = jnp.exp(before_log)
         SR[s] = packed(total, total_log)
-        share(SR.at[s], RR.at[s], 0, back_send.at[s], back_recv.at[s])
+        share_up(s)
 
     def finish(s):
         total = jnp.zeros((LANES, LANES), F32)
@@ -604,13 +633,8 @@
     for s in range(SEQS):
         for k in range(5):
             pair_copy(s, k, c).wait_send()
-        halo(s).wait_send()
-        remote(
-            RS.at[s, 0:3], RS.at[s, 0:3], state_send.at[s], state_recv.at[s], partner
-        ).wait_send()
-        remote(
-            RR.at[s, 0:3], RR.at[s, 0:3], back_send.at[s], back_recv.at[s], partner
-        ).wait_send()
+        pl.when(sp < 15)(halo(s).wait_send)
+        states_out(s)
         remote(
             G.at[s, :, 0:896], G.at[s, :, 0:896], mix_send.at[s], mix_recv.at[s], partner
         ).wait_send()
@@ -674,14 +698,15 @@
             dma((SEQS + 1, 5)),
             dma((SEQS,)),
             dma((SEQS,)),
-            dma((SEQS,)),
-            dma((SEQS,)),
-            dma((SEQS,)),
-            dma((SEQS,)),
+            dma((SEQS, 4)),
+            dma((SEQS, 4)),
+            dma((SEQS, 4)),
+            dma((SEQS, 4)),
             dma((SEQS,)),
             dma((SEQS,)),
             dma((SEQS,)),
             dma((17,)),
+            pltpu.SemaphoreType.REGULAR,
         ],
         compiler_params=pltpu.CompilerParams(
             collective_id=0, has_side_effects=True, vmem_limit_bytes=60 * 1024 * 1024

time: 51.8 us -> 49.5 us (0.956); the launches traced: 51.6 us -> 48.8 us
  Pallas kernels: 50.8 us -> 48 us
    pallas_call x1, Pallas kernels: 50.8 us -> 48 us  [local(): pl.pallas_call(kernel, out_shape=pltpu.VMEM(tokens.shape, BF16), in_specs...]
where the time goes in v7:
time: 49.5 us; the launch traced here: 48.8 us
  Pallas kernels  48 us (97%)
  local copies, waits for them, and re-layouts  0.8 us (2%)
    pallas_call x1, Pallas kernels, local(): pl.pallas_call(kernel, out_shape=pltpu.VMEM(tokens.shape, BF16), in_specs...  48 us

profile of v7, /device:TPU:1, one launch (start us, length us, event | category | flops | bytes accessed | tf_op | source)
XLA Modules:
  0.0 48.8 jit_solution(3267412277297529410)
XLA Ops:
  0.0 48.0 %mixer.1 = bf16[4,64,1024]{2,1,0:T(8,128)(2,1)S(1)} custom-call(f32[2]{0:T(128)} %bias_in.1, f32[2]{0:T(128)} %rate_in.1, bf16[4,64,1024]{2,1,0:T(8,128)(2,1)} %tokens_in.1, f32[1,1024]{1,0:T(1,128)} %bitcast.5, bf16[64,128]{1,0:T(8,128)(2,1)} %xw_in.1, bf16[64,128]{1,0:T(8,128)(2,1)} %zw_in.1, bf16[64,128]{1,0:T(8,128)(2,1)} %bw_in.1, ...), custom_call_target="tpu_custom_call" | custom-call | tf_op jit(solution)/shard_map/mixer/pallas_call | solution.py:661
  48.0 0.8 %copy.16 = bf16[4,64,1024]{2,1,0:T(8,128)(2,1)} copy(bf16[4,64,1024]{2,1,0:T(8,128)(2,1)S(1)} %mixer.1) | data formatting | bytes 1048576

commit v8 on v7

--- a/solution.py
+++ b/solution.py
@@ -157,7 +157,6 @@
     mix_recv,
     local_sem,
     load_sem,
-    ready_sem,
 ):
     z, y = lax.axis_index("sp_0"), lax.axis_index("sp_1")
     x, c = lax.axis_index("tp_0"), lax.axis_index("tp_1")
@@ -181,8 +180,8 @@
         greet(barrier, (z, y, lax.rem(x + step, 4), c))
     greet(barrier, partner)
     for step in (1, 2, 3):
-        pl.when(y + step < 4)(lambda step=step: greet(barrier, (z, y + step, x, c)))
-        pl.when(z + step < 4)(lambda step=step: greet(barrier, (z + step, y, x, c)))
+        greet(barrier, (z, lax.rem(y + step, 4), x, c))
+        greet(barrier, (lax.rem(z + step, 4), y, x, c))
 
     loads = (
         (xw_in, WA.at[z, y, :, 0:128]),
@@ -223,10 +222,7 @@
         ).astype(BF16)
 
     own_columns = pl.multiple_of((c * 4 + x) * LANES, LANES)
-    pl.semaphore_wait(barrier, 3 + y + z)
-    for step in (1, 2, 3):
-        pl.when(y >= step)(lambda step=step: greet(ready_sem, (z, y - step, x, c)))
-        pl.when(z >= step)(lambda step=step: greet(ready_sem, (z - step, y, x, c)))
+    pl.semaphore_wait(barrier, 9)
 
     def token_block(s):
         def block(i, half):
@@ -307,14 +303,12 @@
         pair_copy(s, 3, c).start()
         pair_copy(s, 4, c).start()
 
-    normed(0)
-    token_own(0)
-    pl.when(y + z < 6)(lambda: pl.semaphore_wait(ready_sem, 6 - y - z))
     wa1.own()
     wb1.own()
     wa2[0].own()
     wb2[0].own()
-    oy.own()
+    normed(0)
+    token_own(0)
     normed(1)
     token_own(1)
     normed(2)
@@ -329,21 +323,22 @@
     wa2[2].own()
     wb1.last()
     wb2[2].own()
+    oy.own()
     wa2[0].near()
     wb2[0].near()
     token_near(0)
     token_own(2)
-    token_own(3)
     wa2[1].near()
     wa2[3].near()
     wb2[1].near()
     wb2[3].near()
     token_near(1)
+    token_own(3)
+    wa2[2].near()
+    wb2[2].near()
     oy.near()
     oy.last()
     oz.own()
-    wa2[2].near()
-    wb2[2].near()
     token_last(0)
     wa2[0].last()
     wa2[1].last()
@@ -559,68 +554,68 @@
 
     token_pair(0, 0, 5)
     project(0)
+    token_last(1)
     steps(0)
     conv_tail(0)
     token_near(3)
     oz.near()
     oz.last()
     out_own()
-    token_last(1)
+    token_pair(1, 0, 5)
+    project(1)
     halo_in(0)
     conv_head(0)
     states(0)
     token_last(2)
-    inside(0)
-    gate(0)
-    token_pair(1, 0, 5)
-    project(1)
-    token_last(3)
-    token_pair(2, 0, 5)
-    project(2)
     steps(1)
     conv_tail(1)
+    token_last(3)
     halo_in(1)
     conv_head(1)
     states(1)
+    token_pair(2, 0, 5)
+    project(2)
+    steps(2)
+    conv_tail(2)
     token_pair(3, 0, 5)
     project(3)
-    state_in(0)
-    scan(0)
-    steps(2)
-    conv_tail(2)
     halo_in(2)
     conv_head(2)
     states(2)
+    out_near()
+    state_in(0)
+    scan(0)
     steps(3)
     conv_tail(3)
     halo_in(3)
     conv_head(3)
     states(3)
-    out_near()
     state_in(1)
     scan(1)
+    gate(0)
+    inside(0)
+    gate(1)
+    inside(1)
     back_in(0)
     finish(0)
-    gate(1)
-    inside(1)
+    gate(2)
+    inside(2)
     state_in(2)
     scan(2)
-    gate(2)
-    inside(2)
     gate(3)
     inside(3)
+    back_in(1)
+    finish(1)
     state_in(3)
     scan(3)
-    back_in(1)
-    finish(1)
-    out_last()
     back_in(2)
     finish(2)
     back_in(3)
     finish(3)
-    out_pairs()
+    out_last()
     mixed_in(0)
     mixed_in(1)
+    out_pairs()
     mixed_in(2)
     multiply(0, 3)
     mixed_in(3)
@@ -706,7 +701,6 @@
             dma((SEQS,)),
             dma((SEQS,)),
             dma((17,)),
-            pltpu.SemaphoreType.REGULAR,
         ],
         compiler_params=pltpu.CompilerParams(
             collective_id=0, has_side_effects=True, vmem_limit_bytes=60 * 1024 * 1024

time: 49.5 us -> 48 us (0.970)
  Pallas kernels: 48 us -> 46.6 us
    pallas_call x1, Pallas kernels: 48 us -> 46.6 us  [local(): pl.pallas_call(kernel, out_shape=pltpu.VMEM(tokens.shape, BF16), in_specs...]
where the time goes in v8:
time: 48 us; the launch traced here: 47.4 us
  Pallas kernels  46.6 us (97%)
  local copies, waits for them, and re-layouts  0.8 us (2%)
    pallas_call x1, Pallas kernels, local(): pl.pallas_call(kernel, out_shape=pltpu.VMEM(tokens.shape, BF16), in_specs...  46.6 us

profile of v8, /device:TPU:1, one launch (start us, length us, event | category | flops | bytes accessed | tf_op | source)
XLA Modules:
  0.0 47.4 jit_solution(1894701036679353578)
XLA Ops:
  0.0 46.6 %mixer.1 = bf16[4,64,1024]{2,1,0:T(8,128)(2,1)S(1)} custom-call(f32[2]{0:T(128)} %bias_in.1, f32[2]{0:T(128)} %rate_in.1, bf16[4,64,1024]{2,1,0:T(8,128)(2,1)} %tokens_in.1, f32[1,1024]{1,0:T(1,128)} %bitcast.5, bf16[64,128]{1,0:T(8,128)(2,1)} %xw_in.1, bf16[64,128]{1,0:T(8,128)(2,1)} %zw_in.1, bf16[64,128]{1,0:T(8,128)(2,1)} %bw_in.1, ...), custom_call_target="tpu_custom_call" | custom-call | tf_op jit(solution)/shard_map/mixer/pallas_call | solution.py:656
  46.6 0.8 %copy.16 = bf16[4,64,1024]{2,1,0:T(8,128)(2,1)} copy(bf16[4,64,1024]{2,1,0:T(8,128)(2,1)S(1)} %mixer.1) | data formatting | bytes 1048576

commit v9 on v8

--- a/solution.py
+++ b/solution.py
@@ -37,8 +37,8 @@
 
 
 class Ring:
-    def __init__(self, place, axis, block, sends, recvs, number, direct=False):
-        self.block, self.sends, self.recvs, self.number = block, sends, recvs, number
+    def __init__(self, place, axis, block, send, recvs, both, direct=False):
+        self.block, self.send, self.recvs, self.both = block, send, recvs, both
         self.direct = direct
         self.me = place[axis]
         self.right, self.left = lax.rem(self.me + 1, 4), lax.rem(self.me + 3, 4)
@@ -47,39 +47,22 @@
         self.to_right, self.to_left, self.to_far = to(self.right), to(self.left), to(self.far)
 
     def copy(self, ref, lane, device):
-        return remote(
-            ref, ref, self.sends.at[self.number, lane], self.recvs.at[self.number, lane], device
-        )
+        return remote(ref, ref, self.send, self.recvs.at[lane], device)
 
     def own(self):
         self.copy(self.block(self.me, None), 0, self.to_right).start()
-        self.copy(self.block(self.me, None), 1, self.to_left).start()
+        self.copy(self.block(self.me, None), 0, self.to_left).start()
         if self.direct:
-            self.copy(self.block(self.me, None), 2, self.to_far).start()
+            self.copy(self.block(self.me, None), 1, self.to_far).start()
 
     def near(self):
-        self.copy(self.block(self.left, None), 0, self.to_right).wait_recv()
+        self.copy(self.both, 0, self.to_right).wait_recv()
         if not self.direct:
-            self.copy(self.block(self.left, 0), 2, self.to_right).start()
-        self.copy(self.block(self.right, None), 1, self.to_left).wait_recv()
-        if not self.direct:
-            self.copy(self.block(self.right, 1), 3, self.to_left).start()
+            self.copy(self.block(self.left, 0), 1, self.to_right).start()
+            self.copy(self.block(self.right, 1), 1, self.to_left).start()
 
     def last(self):
-        if self.direct:
-            self.copy(self.block(self.far, None), 2, self.to_far).wait_recv()
-        else:
-            self.copy(self.block(self.far, 0), 2, self.to_right).wait_recv()
-            self.copy(self.block(self.far, 1), 3, self.to_left).wait_recv()
-
-    def drain(self):
-        self.copy(self.block(self.me, None), 0, self.to_right).wait_send()
-        self.copy(self.block(self.me, None), 1, self.to_left).wait_send()
-        if self.direct:
-            self.copy(self.block(self.me, None), 2, self.to_far).wait_send()
-        else:
-            self.copy(self.block(self.left, 0), 2, self.to_right).wait_send()
-            self.copy(self.block(self.right, 1), 3, self.to_left).wait_send()
+        self.copy(self.block(self.far, None), 1, self.to_right).wait_recv()
 
 
 def half_rows(half):
@@ -143,17 +126,12 @@
     ROW,
     GT,
     G,
-    ring_send,
+    sends,
     ring_recv,
-    pair_send,
     pair_recv,
-    halo_send,
     halo_recv,
-    state_send,
     state_recv,
-    back_send,
     back_recv,
-    mix_send,
     mix_recv,
     local_sem,
     load_sem,
@@ -183,24 +161,27 @@
         greet(barrier, (z, lax.rem(y + step, 4), x, c))
         greet(barrier, (lax.rem(z + step, 4), y, x, c))
 
-    loads = (
+    group = lambda k, *pairs: [pltpu.make_async_copy(*pair, load_sem.at[k]) for pair in pairs]
+    weights_in = group(
+        0,
         (xw_in, WA.at[z, y, :, 0:128]),
         (bw_in, WA.at[z, y, :, 128:256]),
         (cw_in, WB.at[z, y, :, 0:128]),
         (zw_in, WB.at[z, y, :, 128:256]),
-        (dw_in, dw_ref),
         (ow_in, OYZ.at[z, y]),
-        (gain_in, gain_ref),
-        *((tokens_in.at[s], tokens_ref.at[s]) for s in range(SEQS)),
-        (xt_in, taps_ref.at[0]),
-        (bt_in, taps_ref.at[1]),
-        (ct_in, taps_ref.at[2]),
-        (og_in, og_ref),
-        (bias_in, bias_ref),
-        (rate_in, rate_ref),
     )
-    loads = [pltpu.make_async_copy(*pair, load_sem.at[k]) for k, pair in enumerate(loads)]
-    for load in loads:
+    (dt_in,) = group(1, (dw_in, dw_ref))
+    (gain_copy,) = group(2, (gain_in, gain_ref))
+    token_copies = [group(3 + s, (tokens_in.at[s], tokens_ref.at[s]))[0] for s in range(SEQS)]
+    taps_in = group(
+        7, *((ref, taps_ref.at[k]) for k, ref in enumerate((xt_in, bt_in, ct_in)))
+    )
+    small_in = [
+        *group(8, (og_in, og_ref)),
+        *group(9, (bias_in, bias_ref)),
+        *group(10, (rate_in, rate_ref)),
+    ]
+    for load in (*weights_in, dt_in, gain_copy, *token_copies, *taps_in, *small_in):
         load.start()
 
     lane = lax.broadcasted_iota(jnp.int32, (1, LANES), 1)
@@ -209,12 +190,14 @@
     head_at = lax.broadcasted_iota(jnp.int32, (2, LANES), 0)
     lane_at = lax.broadcasted_iota(jnp.int32, (2, LANES), 1)
     spread = (lane_at // 64 == head_at).astype(BF16)
-    for load in loads[0:7]:
-        load.wait()
+    five = T.at[0, 0:80, 0:512]
+    pltpu.make_async_copy(five, five, load_sem.at[0]).wait()
+    dt_in.wait()
+    gain_copy.wait()
     WB[z, y, :, 256:384] = matmul(dw_ref[...], spread, ((0,), (0,))).astype(BF16)
 
     def normed(s):
-        loads[7 + s].wait()
+        token_copies[s].wait()
         source = tokens_ref[s].astype(F32)
         scale = lax.rsqrt(jnp.mean(source * source, axis=-1, keepdims=True) + epsilon)
         T[s, pl.ds(pl.multiple_of(tp * ROWS, ROWS), ROWS), :] = (
@@ -232,24 +215,27 @@
 
         return block
 
-    ring = lambda axis, block, number, direct=False: Ring(
-        place, axis, block, ring_send, ring_recv, number, direct
-    )
-    tokens = [ring(2, token_block(s), s) for s in range(SEQS)]
-    wa1 = ring(1, lambda i, h: WA.at[z, i, half_rows(h)], 4, True)
-    wb1 = ring(0, lambda i, h: WB.at[i, y, half_rows(h)], 5, True)
+    def ring(axis, block, number, rows, direct=False):
+        group = 0 if number < SEQS else 1 if number < 16 else 2
+        both = T.at[0, 0:rows, :]
+        send = sends.at[group]
+        return Ring(place, axis, block, send, ring_recv.at[number], both, direct)
+
+    tokens = [ring(2, token_block(s), s, 2 * ROWS) for s in range(SEQS)]
+    wa1 = ring(1, lambda i, h: WA.at[z, i, half_rows(h)], 4, 32, True)
+    wb1 = ring(0, lambda i, h: WB.at[i, y, half_rows(h)], 5, 48, True)
     shifted = lambda i, k: lax.rem(i + k, 4)
-    wa2 = [ring(0, lambda i, h, k=k: WA.at[i, shifted(y, k), half_rows(h)], 6 + k) for k in range(4)]
-    wb2 = [ring(1, lambda i, h, k=k: WB.at[shifted(z, k), i, half_rows(h)], 10 + k) for k in range(4)]
-    oy = ring(1, lambda i, h: OYZ.at[z, i], 14, True)
-    oz = ring(0, lambda i, h: OYZ.at[i], 15, True)
+    wa2 = [ring(0, lambda i, h, k=k: WA.at[i, shifted(y, k), half_rows(h)], 6 + k, 32) for k in range(4)]
+    wb2 = [ring(1, lambda i, h, k=k: WB.at[shifted(z, k), i, half_rows(h)], 10 + k, 48) for k in range(4)]
+    oy = ring(1, lambda i, h: OYZ.at[z, i], 14, 16, True)
+    oz = ring(0, lambda i, h: OYZ.at[i], 15, ROWS, True)
 
     def out_rows(core, i, half):
         rows = LANES if half is None else 64
         start = i * LANES + (0 if half is None else 64 * half)
         return O.at[core, pl.ds(pl.multiple_of(start, 64), rows), :]
 
-    ox = ring(2, lambda i, h: out_rows(c, i, h), 16)
+    ox = ring(2, lambda i, h: out_rows(c, i, h), 16, 256)
 
     def pair_copy(s, k, core):
         i, half = (
@@ -262,12 +248,12 @@
         start = (i * 2 + core) * ROWS + (0 if half is None else 32 * half)
         rows = ROWS if half is None else 32
         ref = T.at[s, pl.ds(pl.multiple_of(start, 32), rows), :]
-        return remote(ref, ref, pair_send.at[s, k], pair_recv.at[s, k], partner)
+        return remote(ref, ref, sends.at[0], pair_recv.at[s], partner)
 
     def out_pair(k, core):
         i, half = ((x, None), (ox.left, None), (ox.right, None), (ox.far, 0), (ox.far, 1))[k]
         ref = out_rows(core, i, half)
-        return remote(ref, ref, pair_send.at[SEQS, k], pair_recv.at[SEQS, k], partner)
+        return remote(ref, ref, sends.at[2], pair_recv.at[SEQS], partner)
 
     def out_own():
         block = OYZ[...].reshape(WIDTH, LANES).astype(F32).T.astype(BF16)
@@ -286,8 +272,7 @@
         out_pair(4, c).start()
 
     def out_pairs():
-        for k in range(5):
-            out_pair(k, other).wait_recv()
+        remote(T.at[0], T.at[0], sends.at[2], pair_recv.at[SEQS], partner).wait_recv()
 
     def token_own(s):
         tokens[s].own()
@@ -350,7 +335,8 @@
     wa2[2].last()
     wb2[2].last()
 
-    for load in loads[11:]:
+    pltpu.make_async_copy(taps_ref, taps_ref, load_sem.at[7]).wait()
+    for load in small_in:
         load.wait()
     bias = jnp.where(low, bias_ref[0], bias_ref[1])
     rate = jnp.where(low, rate_ref[0], rate_ref[1])
@@ -368,53 +354,51 @@
     def share_row(s):
         for k in (1, 3, 2):
             there = (z, lax.rem(y + k, 4), x, c)
-            copy = remote(SS.at[s], RS.at[s, y], state_send.at[s, k], state_recv.at[s, y], there)
+            copy = remote(SS.at[s], RS.at[s, y], sends.at[4], state_recv.at[s], there)
             pl.when((y + k < 4) | (z < 3))(copy.start)
         RS[s, y] = SS[s]
 
     def share_up(s):
         for k in (1, 2, 3):
             there = (lax.rem(z + k, 4), y, x, c)
-            copy = remote(SR.at[s], RR.at[s, z], back_send.at[s, k], back_recv.at[s, z], there)
+            copy = remote(SR.at[s], RR.at[s, z], sends.at[5], back_recv.at[s], there)
             pl.when(z + k < 4)(copy.start)
 
-    def states_out(s):
-        for k in (1, 3, 2):
-            copy = remote(
-                SS.at[s], RS.at[s, y], state_send.at[s, k], state_recv.at[s, y], partner
-            )
-            pl.when((y + k < 4) | (z < 3))(copy.wait_send)
-            copy = remote(SR.at[s], RR.at[s, z], back_send.at[s, k], back_recv.at[s, z], partner)
-            pl.when(z + k < 4)(copy.wait_send)
+    def states_out():
+        for n in (1, 2, 3):
+            ref = RS.at[:, 0:n]
+            copy = remote(ref, ref, sends.at[4], state_recv.at[0], partner)
+            pl.when(jnp.where(z < 3, 3, 3 - y) == n)(copy.wait_send)
+            copy = remote(ref, ref, sends.at[5], back_recv.at[0], partner)
+            pl.when(3 - z == n)(copy.wait_send)
 
     def halo(s):
         return remote(
             E.at[s, :, SPAN : SPAN + 8, :],
             E.at[s, :, 0:8, :],
-            halo_send.at[s],
+            sends.at[3],
             halo_recv.at[s],
             following,
         )
 
-    def token_pair(s, first, last):
-        for k in range(first, last):
-            pair_copy(s, k, other).wait_recv()
+    def token_pair(s):
+        half = T.at[s, 0:256, :]
+        remote(half, half, sends.at[0], pair_recv.at[s], partner).wait_recv()
 
     def halo_in(s):
         pl.when(sp > 0)(halo(s).wait_recv)
 
     def state_in(s):
-        for k in (1, 3, 2):
-            i = lax.rem(y + k, 4)
-            copy = remote(
-                SS.at[s], RS.at[s, i], state_send.at[s, k], state_recv.at[s, i], partner
-            )
-            pl.when((i < y) | (z < 3))(copy.wait_recv)
+        for n in (1, 2, 3):
+            ref = RS.at[s, 0:n]
+            copy = remote(ref, ref, sends.at[4], state_recv.at[s], partner)
+            pl.when(jnp.where(z < 3, 3, y) == n)(copy.wait_recv)
 
     def back_in(s):
-        for i in range(3):
-            copy = remote(SR.at[s], RR.at[s, i], back_send.at[s, 0], back_recv.at[s, i], partner)
-            pl.when(i < z)(copy.wait_recv)
+        for n in (1, 2, 3):
+            ref = RR.at[s, 0:n]
+            copy = remote(ref, ref, sends.at[5], back_recv.at[s], partner)
+            pl.when(z == n)(copy.wait_recv)
 
     def project(s):
         product = matmul(T[s], WA[...].reshape(WIDTH, 256))
@@ -515,24 +499,24 @@
             if k == 0:
                 grown = jnp.exp(CUM[s, CHUNK - 1 : CHUNK, :])
                 entering = grown * (entering + U[s, 0])
-        for rows in tiles:
+        for i in range(8):
+            rows = tiles[i]
             gated = Y[s, rows, :] * jnp.exp(CUM[s, rows, :]) * Z[s, rows, :]
             scale = lax.rsqrt(jnp.mean(gated * gated, axis=-1, keepdims=True) + epsilon)
             GT[s, rows, :] = (gated * scale * og_ref[...]).astype(BF16)
-
-        def send(k, _):
-            i = lax.rem(tp + k, 8)
-            remote(
-                GT.at[s, pl.ds(pl.multiple_of(i * ROWS, ROWS), ROWS), :],
-                G.at[s, :, pl.ds(own_columns, LANES)],
-                mix_send.at[s],
-                mix_recv.at[s],
-                tp_device(i),
-            ).start()
-            return 0
-
-        lax.fori_loop(1, 8, send, 0)
+            if i % 4 == 3:
+                for j in range(i - 3, i + 1):
+                    pl.when(tp != j)(mix_copy(s, j).start)
         own(s).start()
+
+    def mix_copy(s, i):
+        return remote(
+            GT.at[s, i * ROWS : (i + 1) * ROWS, :],
+            G.at[s, :, pl.ds(own_columns, LANES)],
+            sends.at[6],
+            mix_recv.at[s],
+            (z, y, i // 2, i % 2),
+        )
 
     def own(s):
         return pltpu.make_async_copy(
@@ -543,7 +527,7 @@
 
     def mixed_in(s):
         remote(
-            G.at[s, :, 0:896], G.at[s, :, 0:896], mix_send.at[s], mix_recv.at[s], partner
+            G.at[s, :, 0:896], G.at[s, :, 0:896], sends.at[6], mix_recv.at[s], partner
         ).wait_recv()
         own(s).wait()
 
@@ -552,7 +536,22 @@
         result = matmul(gathered, O[...].reshape(WIDTH, WIDTH))
         out_ref[first:last] = result.astype(BF16).reshape(last - first, ROWS, WIDTH)
 
-    token_pair(0, 0, 5)
+    def sent(ref, group):
+        return remote(ref, ref, sends.at[group], pair_recv.at[0], partner)
+
+    def drain():
+        sent(T.at[:, 0:448, :], 0).wait_send()
+        sent(T.at[0:3, 0:240, :], 1).wait_send()
+        pl.when(sp < 15)(sent(E.at[:, :, 0:8, :], 3).wait_send)
+        states_out()
+
+    def ox_drain():
+        sent(T.at[0:2, 0:448, :], 2).wait_send()
+
+    def out_drain():
+        sent(G.at[:, :, 0:896], 6).wait_send()
+
+    token_pair(0)
     project(0)
     token_last(1)
     steps(0)
@@ -561,23 +560,23 @@
     oz.near()
     oz.last()
     out_own()
-    token_pair(1, 0, 5)
+    token_pair(1)
     project(1)
+    token_last(2)
     halo_in(0)
     conv_head(0)
     states(0)
-    token_last(2)
     steps(1)
     conv_tail(1)
-    token_last(3)
     halo_in(1)
     conv_head(1)
     states(1)
-    token_pair(2, 0, 5)
+    token_last(3)
+    token_pair(2)
     project(2)
     steps(2)
     conv_tail(2)
-    token_pair(3, 0, 5)
+    token_pair(3)
     project(3)
     halo_in(2)
     conv_head(2)
@@ -613,26 +612,17 @@
     back_in(3)
     finish(3)
     out_last()
+    drain()
     mixed_in(0)
     mixed_in(1)
     out_pairs()
+    ox_drain()
+    multiply(0, 2)
     mixed_in(2)
-    multiply(0, 3)
     mixed_in(3)
-    multiply(3, 4)
-
-    for each in (*tokens, wa1, wb1, *wa2, *wb2, oy, oz, ox):
-        each.drain()
-    for k in range(5):
-        out_pair(k, c).wait_send()
-    for s in range(SEQS):
-        for k in range(5):
-            pair_copy(s, k, c).wait_send()
-        pl.when(sp < 15)(halo(s).wait_send)
-        states_out(s)
-        remote(
-            G.at[s, :, 0:896], G.at[s, :, 0:896], mix_send.at[s], mix_recv.at[s], partner
-        ).wait_send()
+    multiply(2, 4)
+
+    out_drain()
 
 
 def local(
@@ -687,20 +677,15 @@
             pltpu.VMEM((SEQS, LANES + 8, LANES), F32),
             pltpu.VMEM((SEQS, SPAN, LANES), BF16),
             pltpu.VMEM((SEQS, ROWS, WIDTH), BF16),
-            dma((17, 4)),
-            dma((17, 4)),
-            dma((SEQS + 1, 5)),
-            dma((SEQS + 1, 5)),
-            dma((SEQS,)),
-            dma((SEQS,)),
-            dma((SEQS, 4)),
-            dma((SEQS, 4)),
-            dma((SEQS, 4)),
-            dma((SEQS, 4)),
+            dma((7,)),
+            dma((17, 2)),
+            dma((SEQS + 1,)),
             dma((SEQS,)),
             dma((SEQS,)),
             dma((SEQS,)),
-            dma((17,)),
+            dma((SEQS,)),
+            dma((SEQS,)),
+            dma((11,)),
         ],
         compiler_params=pltpu.CompilerParams(
             collective_id=0, has_side_effects=True, vmem_limit_bytes=60 * 1024 * 1024

time: 48 us -> 45.5 us (0.948)
  Pallas kernels: 46.6 us -> 44.3 us
    pallas_call x1, Pallas kernels: 46.6 us -> 44.3 us  [local(): pl.pallas_call(kernel, out_shape=pltpu.VMEM(tokens.shape, BF16), in_specs...]
where the time goes in v9:
time: 45.5 us; the launch traced here: 45.1 us
  Pallas kernels  44.3 us (97%)
  local copies, waits for them, and re-layouts  0.8 us (2%)
    pallas_call x1, Pallas kernels, local(): pl.pallas_call(kernel, out_shape=pltpu.VMEM(tokens.shape, BF16), in_specs...  44.3 us

profile of v9, /device:TPU:1, one launch (start us, length us, event | category | flops | bytes accessed | tf_op | source)
XLA Modules:
  0.0 45.1 jit_solution(12985504368378357107)
XLA Ops:
  0.0 44.3 %mixer.1 = bf16[4,64,1024]{2,1,0:T(8,128)(2,1)S(1)} custom-call(f32[2]{0:T(128)} %bias_in.1, f32[2]{0:T(128)} %rate_in.1, bf16[4,64,1024]{2,1,0:T(8,128)(2,1)} %tokens_in.1, f32[1,1024]{1,0:T(1,128)} %bitcast.5, bf16[64,128]{1,0:T(8,128)(2,1)} %xw_in.1, bf16[64,128]{1,0:T(8,128)(2,1)} %zw_in.1, bf16[64,128]{1,0:T(8,128)(2,1)} %bw_in.1, ...), custom_call_target="tpu_custom_call" | custom-call | tf_op jit(solution)/shard_map/mixer/pallas_call | solution.py:646
  44.3 0.8 %copy.16 = bf16[4,64,1024]{2,1,0:T(8,128)(2,1)} copy(bf16[4,64,1024]{2,1,0:T(8,128)(2,1)S(1)} %mixer.1) | data formatting | bytes 1048576

commit v10 on v9

--- a/solution.py
+++ b/solution.py
@@ -47,7 +47,7 @@
         self.to_right, self.to_left, self.to_far = to(self.right), to(self.left), to(self.far)
 
     def copy(self, ref, lane, device):
-        return remote(ref, ref, self.send, self.recvs.at[lane], device)
+        return remote(ref, ref, self.send, self.recvs[lane], device)
 
     def own(self):
         self.copy(self.block(self.me, None), 0, self.to_right).start()
@@ -205,6 +205,7 @@
         ).astype(BF16)
 
     own_columns = pl.multiple_of((c * 4 + x) * LANES, LANES)
+    normed(0)
     pl.semaphore_wait(barrier, 9)
 
     def token_block(s):
@@ -219,14 +220,16 @@
         group = 0 if number < SEQS else 1 if number < 16 else 2
         both = T.at[0, 0:rows, :]
         send = sends.at[group]
-        return Ring(place, axis, block, send, ring_recv.at[number], both, direct)
+        last = number if number < 6 else max(6, number - 7)
+        recvs = (ring_recv.at[number], ring_recv.at[17 + last])
+        return Ring(place, axis, block, send, recvs, both, direct)
 
     tokens = [ring(2, token_block(s), s, 2 * ROWS) for s in range(SEQS)]
     wa1 = ring(1, lambda i, h: WA.at[z, i, half_rows(h)], 4, 32, True)
     wb1 = ring(0, lambda i, h: WB.at[i, y, half_rows(h)], 5, 48, True)
     shifted = lambda i, k: lax.rem(i + k, 4)
-    wa2 = [ring(0, lambda i, h, k=k: WA.at[i, shifted(y, k), half_rows(h)], 6 + k, 32) for k in range(4)]
-    wb2 = [ring(1, lambda i, h, k=k: WB.at[shifted(z, k), i, half_rows(h)], 10 + k, 48) for k in range(4)]
+    wa2 = [ring(0, lambda i, h, k=k: WA.at[i, shifted(y, k), half_rows(h)], 6 + k, 32, k in (2,)) for k in range(4)]
+    wb2 = [ring(1, lambda i, h, k=k: WB.at[shifted(z, k), i, half_rows(h)], 10 + k, 48, k in (2,)) for k in range(4)]
     oy = ring(1, lambda i, h: OYZ.at[z, i], 14, 16, True)
     oz = ring(0, lambda i, h: OYZ.at[i], 15, ROWS, True)
 
@@ -292,7 +295,6 @@
     wb1.own()
     wa2[0].own()
     wb2[0].own()
-    normed(0)
     token_own(0)
     normed(1)
     token_own(1)
@@ -325,15 +327,9 @@
     oy.last()
     oz.own()
     token_last(0)
-    wa2[0].last()
-    wa2[1].last()
-    wa2[3].last()
-    wb2[0].last()
-    wb2[1].last()
-    wb2[3].last()
     token_near(2)
-    wa2[2].last()
-    wb2[2].last()
+    weights = T.at[0, 0:160, :]
+    remote(weights, weights, sends.at[1], ring_recv.at[23], partner).wait_recv()
 
     pltpu.make_async_copy(taps_ref, taps_ref, load_sem.at[7]).wait()
     for load in small_in:
@@ -412,7 +408,7 @@
 
     def gate(s):
         for rows in tiles:
-            Z[s, rows, :] = silu(Z[s, rows, :])
+            Z[s, rows, :] = silu(Z[s, rows, :]) * jnp.exp(CUM[s, rows, :])
 
     def steps(s):
         for rows in tiles:
@@ -467,7 +463,11 @@
             rows = slice(k * CHUNK, (k + 1) * CHUNK)
             scores = matmul(CS[s, rows, :], BS[s, rows, :], ((1,), (1,)))
             scores = jnp.where(lower, scores, 0.0).astype(BF16)
-            Y[s, rows, :] = matmul(scores, XS[s, rows, :])
+            part = matmul(scores, XS[s, rows, :])
+            if k:
+                grown = jnp.exp(CUM[s, CHUNK - 1 : CHUNK, :])
+                part = part + grown * matmul(CS[s, rows, :], U[s, 0].astype(BF16))
+            Y[s, rows, :] = part
 
     def scan(s):
         before, before_log = jnp.zeros((LANES, LANES), F32), jnp.zeros((1, LANES), F32)
@@ -493,15 +493,12 @@
             total = jnp.exp(piece[LANES : LANES + 1]) * total + piece[0:LANES]
             entering = jnp.where(i + 1 == z, total, entering)
         entering = ROW[s, LANES : LANES + 1] * entering + ROW[s, 0:LANES]
-        for k in range(2):
-            rows = slice(k * CHUNK, (k + 1) * CHUNK)
-            Y[s, rows, :] += matmul(CS[s, rows, :], entering.astype(BF16))
-            if k == 0:
-                grown = jnp.exp(CUM[s, CHUNK - 1 : CHUNK, :])
-                entering = grown * (entering + U[s, 0])
+        carried = matmul(CS[s], entering.astype(BF16))
+        grown = jnp.exp(CUM[s, CHUNK - 1 : CHUNK, :])
         for i in range(8):
             rows = tiles[i]
-            gated = Y[s, rows, :] * jnp.exp(CUM[s, rows, :]) * Z[s, rows, :]
+            part = carried[rows] if i < 4 else grown * carried[rows]
+            gated = (Y[s, rows, :] + part) * Z[s, rows, :]
             scale = lax.rsqrt(jnp.mean(gated * gated, axis=-1, keepdims=True) + epsilon)
             GT[s, rows, :] = (gated * scale * og_ref[...]).astype(BF16)
             if i % 4 == 3:
@@ -514,7 +511,7 @@
             GT.at[s, i * ROWS : (i + 1) * ROWS, :],
             G.at[s, :, pl.ds(own_columns, LANES)],
             sends.at[6],
-            mix_recv.at[s],
+            mix_recv.at[s // 2],
             (z, y, i // 2, i % 2),
         )
 
@@ -522,14 +519,16 @@
         return pltpu.make_async_copy(
             GT.at[s, pl.ds(pl.multiple_of(tp * ROWS, ROWS), ROWS), :],
             G.at[s, :, pl.ds(own_columns, LANES)],
-            local_sem.at[s],
+            local_sem.at[0],
         )
 
-    def mixed_in(s):
-        remote(
-            G.at[s, :, 0:896], G.at[s, :, 0:896], sends.at[6], mix_recv.at[s], partner
-        ).wait_recv()
-        own(s).wait()
+    def mixed_in(pair):
+        ref = G.at[2 * pair : 2 * pair + 2, :, 0:896]
+        remote(ref, ref, sends.at[6], mix_recv.at[pair], partner).wait_recv()
+
+    def owns_in():
+        ref = G.at[:, :, 0:LANES]
+        pltpu.make_async_copy(ref, ref, local_sem.at[0]).wait()
 
     def multiply(first, last):
         gathered = G[first:last].reshape((last - first) * ROWS, WIDTH)
@@ -613,13 +612,12 @@
     finish(3)
     out_last()
     drain()
+    owns_in()
     mixed_in(0)
-    mixed_in(1)
     out_pairs()
     ox_drain()
     multiply(0, 2)
-    mixed_in(2)
-    mixed_in(3)
+    mixed_in(1)
     multiply(2, 4)
 
     out_drain()
@@ -678,13 +676,13 @@
             pltpu.VMEM((SEQS, SPAN, LANES), BF16),
             pltpu.VMEM((SEQS, ROWS, WIDTH), BF16),
             dma((7,)),
-            dma((17, 2)),
+            dma((27,)),
             dma((SEQS + 1,)),
             dma((SEQS,)),
             dma((SEQS,)),
             dma((SEQS,)),
-            dma((SEQS,)),
-            dma((SEQS,)),
+            dma((2,)),
+            dma((1,)),
             dma((11,)),
         ],
         compiler_params=pltpu.CompilerParams(

time: 45.5 us -> 45.2 us (level)
  no operation moved by 1% of the time
where the time goes in v10:
time: 45.2 us; the launch traced here: 44.7 us
  Pallas kernels  43.9 us (97%)
  local copies, waits for them, and re-layouts  0.8 us (2%)
    pallas_call x1, Pallas kernels, local(): pl.pallas_call(kernel, out_shape=pltpu.VMEM(tokens.shape, BF16), in_specs...  43.9 us

profile of v10, /device:TPU:1, one launch (start us, length us, event | category | flops | bytes accessed | tf_op | source)
XLA Modules:
  0.0 44.7 jit_solution(173141662354862695)
XLA Ops:
  0.0 43.9 %mixer.1 = bf16[4,64,1024]{2,1,0:T(8,128)(2,1)S(1)} custom-call(f32[2]{0:T(128)} %bias_in.1, f32[2]{0:T(128)} %rate_in.1, bf16[4,64,1024]{2,1,0:T(8,128)(2,1)} %tokens_in.1, f32[1,1024]{1,0:T(1,128)} %bitcast.5, bf16[64,128]{1,0:T(8,128)(2,1)} %xw_in.1, bf16[64,128]{1,0:T(8,128)(2,1)} %zw_in.1, bf16[64,128]{1,0:T(8,128)(2,1)} %bw_in.1, ...), custom_call_target="tpu_custom_call" | custom-call | tf_op jit(solution)/shard_map/mixer/pallas_call | solution.py:644
  43.9 0.8 %copy.16 = bf16[4,64,1024]{2,1,0:T(8,128)(2,1)} copy(bf16[4,64,1024]{2,1,0:T(8,128)(2,1)S(1)} %mixer.1) | data formatting | bytes 1048576

commit v11 on v10

--- a/solution.py
+++ b/solution.py
@@ -317,10 +317,10 @@
     token_own(2)
     wa2[1].near()
     wa2[3].near()
+    token_near(1)
+    token_own(3)
     wb2[1].near()
     wb2[3].near()
-    token_near(1)
-    token_own(3)
     wa2[2].near()
     wb2[2].near()
     oy.near()

time: 45.2 us -> 45.2 us (level)
  no operation moved by 1% of the time
where the time goes in v11:
time: 45.2 us; the launch traced here: 44.7 us
  Pallas kernels  43.9 us (97%)
  local copies, waits for them, and re-layouts  0.8 us (2%)
    pallas_call x1, Pallas kernels, local(): pl.pallas_call(kernel, out_shape=pltpu.VMEM(tokens.shape, BF16), in_specs...  43.9 us

profile of v11, /device:TPU:1, one launch (start us, length us, event | category | flops | bytes accessed | tf_op | source)
XLA Modules:
  0.0 44.7 jit_solution(363101946328145147)
XLA Ops:
  0.0 43.9 %mixer.1 = bf16[4,64,1024]{2,1,0:T(8,128)(2,1)S(1)} custom-call(f32[2]{0:T(128)} %bias_in.1, f32[2]{0:T(128)} %rate_in.1, bf16[4,64,1024]{2,1,0:T(8,128)(2,1)} %tokens_in.1, f32[1,1024]{1,0:T(1,128)} %bitcast.5, bf16[64,128]{1,0:T(8,128)(2,1)} %xw_in.1, bf16[64,128]{1,0:T(8,128)(2,1)} %zw_in.1, bf16[64,128]{1,0:T(8,128)(2,1)} %bw_in.1, ...), custom_call_target="tpu_custom_call" | custom-call | tf_op jit(solution)/shard_map/mixer/pallas_call | solution.py:644
  43.9 0.8 %copy.16 = bf16[4,64,1024]{2,1,0:T(8,128)(2,1)} copy(bf16[4,64,1024]{2,1,0:T(8,128)(2,1)S(1)} %mixer.1) | data formatting | bytes 1048576

commit v12 on v11

--- a/solution.py
+++ b/solution.py
@@ -172,14 +172,14 @@
     )
     (dt_in,) = group(1, (dw_in, dw_ref))
     (gain_copy,) = group(2, (gain_in, gain_ref))
-    token_copies = [group(3 + s, (tokens_in.at[s], tokens_ref.at[s]))[0] for s in range(SEQS)]
+    token_copies = group(3, (tokens_in, tokens_ref))
     taps_in = group(
-        7, *((ref, taps_ref.at[k]) for k, ref in enumerate((xt_in, bt_in, ct_in)))
+        4, *((ref, taps_ref.at[k]) for k, ref in enumerate((xt_in, bt_in, ct_in)))
     )
     small_in = [
-        *group(8, (og_in, og_ref)),
-        *group(9, (bias_in, bias_ref)),
-        *group(10, (rate_in, rate_ref)),
+        *group(5, (og_in, og_ref)),
+        *group(6, (bias_in, bias_ref)),
+        *group(7, (rate_in, rate_ref)),
     ]
     for load in (*weights_in, dt_in, gain_copy, *token_copies, *taps_in, *small_in):
         load.start()
@@ -197,7 +197,8 @@
     WB[z, y, :, 256:384] = matmul(dw_ref[...], spread, ((0,), (0,))).astype(BF16)
 
     def normed(s):
-        token_copies[s].wait()
+        if s == 0:
+            token_copies[0].wait()
         source = tokens_ref[s].astype(F32)
         scale = lax.rsqrt(jnp.mean(source * source, axis=-1, keepdims=True) + epsilon)
         T[s, pl.ds(pl.multiple_of(tp * ROWS, ROWS), ROWS), :] = (
@@ -331,7 +332,7 @@
     weights = T.at[0, 0:160, :]
     remote(weights, weights, sends.at[1], ring_recv.at[23], partner).wait_recv()
 
-    pltpu.make_async_copy(taps_ref, taps_ref, load_sem.at[7]).wait()
+    pltpu.make_async_copy(taps_ref, taps_ref, load_sem.at[4]).wait()
     for load in small_in:
         load.wait()
     bias = jnp.where(low, bias_ref[0], bias_ref[1])
@@ -577,14 +578,14 @@
     conv_tail(2)
     token_pair(3)
     project(3)
+    steps(3)
+    conv_tail(3)
     halo_in(2)
     conv_head(2)
     states(2)
     out_near()
     state_in(0)
     scan(0)
-    steps(3)
-    conv_tail(3)
     halo_in(3)
     conv_head(3)
     states(3)
@@ -683,7 +684,7 @@
             dma((SEQS,)),
             dma((2,)),
             dma((1,)),
-            dma((11,)),
+            dma((8,)),
         ],
         compiler_params=pltpu.CompilerParams(
             collective_id=0, has_side_effects=True, vmem_limit_bytes=60 * 1024 * 1024

time: 45.2 us -> 45.4 us (level)
  no operation moved by 1% of the time
where the time goes in v12:
time: 45.4 us; the launch traced here: 45 us
  Pallas kernels  44.2 us (97%)
  local copies, waits for them, and re-layouts  0.8 us (2%)
    pallas_call x1, Pallas kernels, local(): pl.pallas_call(kernel, out_shape=pltpu.VMEM(tokens.shape, BF16), in_specs...  44.2 us

profile of v12, /device:TPU:1, one launch (start us, length us, event | category | flops | bytes accessed | tf_op | source)
XLA Modules:
  0.0 45.0 jit_solution(9030758331101002220)
XLA Ops:
  0.0 44.2 %mixer.1 = bf16[4,64,1024]{2,1,0:T(8,128)(2,1)S(1)} custom-call(f32[2]{0:T(128)} %bias_in.1, f32[2]{0:T(128)} %rate_in.1, bf16[4,64,1024]{2,1,0:T(8,128)(2,1)} %tokens_in.1, f32[1,1024]{1,0:T(1,128)} %bitcast.5, bf16[64,128]{1,0:T(8,128)(2,1)} %xw_in.1, bf16[64,128]{1,0:T(8,128)(2,1)} %zw_in.1, bf16[64,128]{1,0:T(8,128)(2,1)} %bw_in.1, ...), custom_call_target="tpu_custom_call" | custom-call | tf_op jit(solution)/shard_map/mixer/pallas_call | solution.py:645
  44.2 0.8 %copy.16 = bf16[4,64,1024]{2,1,0:T(8,128)(2,1)} copy(bf16[4,64,1024]{2,1,0:T(8,128)(2,1)S(1)} %mixer.1) | data formatting | bytes 1048576
